TPU v7x, 256 devices: a 4x2x16 block of a 4x16x16 slice. The times are simulated.
256 devices in a mesh: grp: 2 (over y), sp: 32 (over z, core), tp: 4 (over x).
Axes of the slice: x: 4, y: 2, z: 16, core: 2. Of those that a mesh axis runs over, the one named last changes fastest.
The devices are a block of a 4x16x16 slice.
Arguments:
- latents: bfloat16 [32768, 2048], P(('grp', 'sp', 'tp')), parts along dimension 0, may hold values from -6 to 6
- conv_value: bfloat16 [32768, 1024], P(('grp', 'sp'), 'tp'), parts along dimension 0, may hold values from -6 to 6
- conv_gate: bfloat16 [32768, 1024], P(('grp', 'sp'), 'tp'), parts along dimension 0, may hold values from -6 to 6
- conv_taps: float32 [31, 1024], P(None, 'tp'), may hold values from -2.2 to 2.2
- conv_gain: float32 [1024], P('tp'), may hold values from 0.1 to 1.9
- point_weight: bfloat16 [1024, 2048], P('tp'), may hold values from -0.1875 to 0.1875
- channel_gain: float32 [2048], replicated, may hold values from 0.1 to 1.9
- expert_ids: int32 [32768, 2], P(('grp', 'sp', 'tp')), parts along dimension 0, may hold values from 0 to 127, all different within a row; in each aligned block of 128 rows (0 to 127, 128 to 255, ...) at most 4 rows name the same one
- expert_weights: float32 [32768, 2], P(('grp', 'sp', 'tp')), parts along dimension 0, may hold values from 0.2 to 1
- gate_weight: bfloat16 [128, 2048, 768], P(('sp', 'tp')), may hold values from -0.125 to 0.125
- up_weight: bfloat16 [128, 2048, 768], P(('sp', 'tp')), may hold values from -0.125 to 0.125
- down_weight: bfloat16 [128, 768, 2048], P(('sp', 'tp')), may hold values from -0.21875 to 0.21875
Outputs:
- result: bfloat16 [32768, 2048], P(('grp', 'sp', 'tp')), parts along dimension 0
There are 2 independent parts, one for each index of `grp`. A program takes and returns all parts, laid end to end along the dimension named above; an argument that names none is the same for every part. Nothing has to cross between parts.
Inputs may be any that keep to these rules, and one draw needn't show every extreme that they name: `expert_ids`: each row names 2 different experts. Within the rows of one device (aligned blocks of 128 rows) no expert is named by more than 4 rows, and in some device's rows some expert is named by exactly 4.
All inputs are finite; a program needn't handle non-finite values.
Results may differ from a plain program's by a relative error of at most 0.012.
Values may be sent and summed in bfloat16 or wider, within the bound.
No kernel may reach another device: no remote copies, remote signals or barrier semaphores. Data moves between devices by JAX's collectives and lax.ppermute only.
A program may use at most 64 MiB of HBM per device.

v0:
```python
import jax
import jax.numpy as jnp
from jax import lax
from jax.experimental import pallas as pl
from jax.experimental.pallas import tpu as pltpu
from jax.sharding import PartitionSpec as P


F32 = jnp.float32
BF16 = jnp.bfloat16
HALO = 16
LANES = 128
PACK = 8


def dot(a, b):
    return jnp.dot(a, b, preferred_element_type=F32)


def iota(shape, dim):
    return lax.broadcasted_iota(jnp.int32, shape, dim)


def gate(value, gating):
    return (value.astype(F32) * jax.nn.sigmoid(gating.astype(F32))).astype(BF16)


def conv_kernel(rows_ref, low_ref, high_ref, table_ref, out_ref, pad_ref):
    taps, width = table_ref.shape[0] - 1, table_ref.shape[1]
    rows = rows_ref.shape[0]
    owners, owner_rows = out_ref.shape[0], out_ref.shape[1] - PACK
    step = 64
    parts = [slice(first, first + LANES) for first in range(0, width, LANES)]
    for part, lanes in enumerate(parts):
        pad_ref[part, 0:HALO] = low_ref[:, lanes].astype(F32)
        pad_ref[part, HALO : HALO + rows] = rows_ref[:, lanes].astype(F32)
        pad_ref[part, HALO + rows :] = high_ref[:, lanes].astype(F32)
    for part, lanes in enumerate(parts):
        for start in range(0, rows, step):
            total = jnp.zeros((step, LANES), F32)
            for tap in range(taps):
                first = start + HALO - taps // 2 + tap
                total = total + table_ref[tap : tap + 1, lanes] * pad_ref[part, first : first + step]
            owner, row = divmod(start, owner_rows)
            out_ref[owner, row : row + step, lanes] = total
    for owner in range(owners):
        out_ref[owner, owner_rows:, :] = jnp.broadcast_to(table_ref[taps:, :], (PACK, width))


def slots(ids_ref, experts):
    tokens = ids_ref.shape[1]
    expert = iota((experts, tokens), 0)
    chosen = jnp.zeros((experts, tokens), F32)
    for k in range(ids_ref.shape[0]):
        chosen = jnp.where(ids_ref[k : k + 1, :] == expert, 1.0, chosen)
    before = (iota((tokens, tokens), 0) < iota((tokens, tokens), 1)).astype(F32).astype(BF16)
    earlier = dot(chosen.astype(BF16), before)
    return jnp.where(chosen > 0, earlier + 1.0, 0.0)


def dispatch_kernel(
    place_ref, mixed_ref, latents_ref, own_ref, near_ref, swapped_ref, half_ref, rest_ref, gain_ref, ids_ref, after_ref, box_ref, act_ref, x_ref,
):
    owners, _, width = mixed_ref.shape
    rows, features = latents_ref.shape
    half_width = width // 2
    total = jnp.zeros((rows, 1), F32)
    squares = jnp.zeros((rows, 1), F32)
    for j in range(owners):
        block = mixed_ref[j, :rows, :]
        total = total + jnp.sum(block, axis=1, keepdims=True)
        squares = squares + jnp.sum(block * block, axis=1, keepdims=True)
    center = total / (owners * width)
    scale = lax.rsqrt(squares / (owners * width) - center * center + 0.05)
    for j in range(owners):
        value = (mixed_ref[j, :rows, :] - center) * scale * mixed_ref[j, rows : rows + 1, :]
        act_ref[j] = (value * jax.nn.sigmoid(value)).astype(BF16)
    place, core = place_ref[0], place_ref[1]
    before = lax.rem(place + owners - 1 + 2 * core, owners)
    beyond = lax.rem(place + owners + 1 - 2 * core, owners)
    across = act_ref[lax.rem(place + 2, owners)]
    lower, upper = across[:, :half_width], across[:, half_width:]
    first = jnp.where(core == 0, lower, upper)
    second = jnp.where(core == 0, upper, lower)
    step = 512
    squares = jnp.zeros((rows, 1), F32)
    for start in range(0, features, step):
        cols = slice(start, start + step)
        branch = dot(act_ref[place], own_ref[:, cols])
        branch = branch + dot(act_ref[before], near_ref[:, cols])
        branch = branch + dot(act_ref[beyond], swapped_ref[:, cols])
        branch = branch + dot(first, half_ref[:, cols]) + dot(second, rest_ref[:, cols])
        after = (latents_ref[:, cols].astype(F32) + branch).astype(BF16)
        after_ref[:, cols] = after
        after = after.astype(F32)
        squares = squares + jnp.sum(after * after, axis=1, keepdims=True)
    scale = lax.rsqrt(squares / features + 0.01)
    parts, cap = x_ref.shape[0] // rows, PACK * rows // x_ref.shape[0]
    span = features // parts
    for part in range(parts):
        cols = slice(part * span, (part + 1) * span)
        value = after_ref[:, cols].astype(F32) * scale * gain_ref[:, cols]
        x_ref[part * rows : (part + 1) * rows] = value.astype(BF16)
    experts = box_ref.shape[0] // PACK
    slot = slots(ids_ref, experts).astype(BF16)
    block = 2 * LANES
    for start in range(0, box_ref.shape[0], block):
        row = iota((block, experts), 0) + start
        spread = ((row >> 3) == iota((block, experts), 1)).astype(F32).astype(BF16)
        wanted = dot(spread, slot)
        row = iota((block, rows), 0)
        hit = wanted == ((row & (cap - 1)) + 1).astype(F32)
        picks = [
            (hit & (((row & (PACK - 1)) // cap) == part)).astype(F32).astype(BF16)
            for part in range(parts)
        ]
        pick = jnp.concatenate(picks, axis=1)
        box_ref[start : start + block] = dot(pick, x_ref[...]).astype(BF16)


def shuffle_matrix(size, parts, inverse):
    cap = PACK // parts
    sources = size // PACK
    packed = iota((size, size), 0 if inverse else 1)
    split = iota((size, size), 1 if inverse else 0)
    source, part, slot = packed >> 3, (packed & (PACK - 1)) // cap, packed & (cap - 1)
    return ((part * sources + source) * cap + slot == split).astype(F32).astype(BF16)


def expert_kernel(in_ref, gate_ref, up_ref, down_ref, out_ref, x_ref, hidden_ref, y_ref):
    parts, rows, span = x_ref.shape
    block = 2 * LANES
    sub = block // parts
    forward = shuffle_matrix(block, parts, False)
    for i in range(in_ref.shape[0] // block):
        moved = dot(forward, in_ref[i * block : (i + 1) * block]).astype(BF16)
        for part in range(parts):
            x_ref[part, i * sub : (i + 1) * sub] = moved[part * sub : (part + 1) * sub]
    hidden_width = gate_ref.shape[1]
    tile = 256

    def inner(n, carry):
        cols = pl.ds(pl.multiple_of(n * tile, tile), tile)
        gated = jnp.zeros((rows, tile), F32)
        upped = jnp.zeros((rows, tile), F32)
        for part in range(parts):
            at = slice(part * span, (part + 1) * span)
            gated = gated + dot(x_ref[part], gate_ref[at, cols])
            upped = upped + dot(x_ref[part], up_ref[at, cols])
        hidden_ref[:, cols] = (gated * jax.nn.sigmoid(gated) * upped).astype(BF16)
        return carry

    lax.fori_loop(0, hidden_width // tile, inner, 0)
    for part in range(parts):

        def outer(n, carry, part=part):
            cols = pl.ds(pl.multiple_of(n * tile, tile), tile)
            weights = down_ref[:, pl.ds(pl.multiple_of(part * span + n * tile, tile), tile)]
            y_ref[part, :, cols] = dot(hidden_ref[...], weights).astype(BF16)
            return carry

        lax.fori_loop(0, span // tile, outer, 0)
    backward = shuffle_matrix(block, parts, True)
    for i in range(in_ref.shape[0] // block):
        stacked = jnp.concatenate(
            [y_ref[part, i * sub : (i + 1) * sub] for part in range(parts)], axis=0
        )
        out_ref[i * block : (i + 1) * block] = dot(backward, stacked).astype(BF16)


def combine_kernel(in_ref, after_ref, ids_ref, weights_ref, out_ref):
    rows, features = after_ref.shape
    size, span = in_ref.shape
    parts = features // span
    cap = PACK // parts
    experts = size // PACK
    slot = jnp.transpose(slots(ids_ref, experts)).astype(BF16)
    expert = iota((experts, rows), 0)
    weight = jnp.zeros((experts, rows), F32)
    for k in range(ids_ref.shape[0]):
        weight = jnp.where(ids_ref[k : k + 1, :] == expert, weights_ref[k : k + 1, :], weight)
    weight = jnp.transpose(weight)
    coarse = weight.astype(BF16)
    fine = (weight - coarse.astype(F32)).astype(BF16)
    spread = (iota((experts, size), 0) == (iota((experts, size), 1) >> 3)).astype(F32).astype(BF16)
    column = iota((rows, size), 1)
    hit = dot(slot, spread) == ((column & (cap - 1)) + 1).astype(F32)
    coarse = jnp.where(hit, dot(coarse, spread), 0.0)
    fine = jnp.where(hit, dot(fine, spread), 0.0)
    for part in range(parts):
        here = ((column & (PACK - 1)) // cap) == part
        factors = jnp.concatenate(
            [jnp.where(here, coarse, 0.0).astype(BF16), jnp.where(here, fine, 0.0).astype(BF16)], axis=0
        )
        sums = dot(factors, in_ref[...])
        cols = slice(part * span, (part + 1) * span)
        out_ref[:, cols] = (after_ref[:, cols].astype(F32) + (sums[:rows] + sums[rows:])).astype(BF16)


VMEM = pl.BlockSpec(memory_space=pltpu.VMEM)
SMEM = pl.BlockSpec(memory_space=pltpu.SMEM)


def call(kernel, specs, outs, scratch, flops, size):
    return pl.pallas_call(
        kernel,
        in_specs=specs,
        out_specs=VMEM if not isinstance(outs, (list, tuple)) else [VMEM] * len(outs),
        out_shape=outs,
        scratch_shapes=scratch,
        compiler_params=pltpu.CompilerParams(vmem_limit_bytes=size << 20),
        cost_estimate=pl.CostEstimate(flops=flops, bytes_accessed=1 << 20, transcendentals=0),
    )


def shards(
    latents, conv_value, conv_gate, conv_taps, conv_gain, point_weight, channel_gain,
    expert_ids, expert_weights, gate_weight, up_weight, down_weight,
):
    shape = jax.ShapeDtypeStruct
    rows, features = latents.shape
    block_rows, width = conv_value.shape
    owners = lax.axis_size("tp")
    stages = lax.axis_size("sp")
    members = owners * stages
    top_count = expert_ids.shape[1]
    experts = gate_weight.shape[0] * members
    cap = 2 * top_count * rows // experts
    parts = PACK // cap
    span = features // parts

    ahead = [(i, i + 1) for i in range(stages - 1)]
    behind = [(i + 1, i) for i in range(stages - 1)]
    low = lax.ppermute(gate(conv_value[-HALO:], conv_gate[-HALO:]), "sp", ahead)
    high = lax.ppermute(gate(conv_value[:HALO], conv_gate[:HALO]), "sp", behind)

    place = lax.axis_index("tp")
    core = lax.rem(lax.axis_index("sp"), 2)
    half_width = width // 2
    aside = [
        (stage * owners + i, stage * owners + (i + (1, owners - 1)[stage % 2]) % owners)
        for stage in range(stages)
        for i in range(owners)
    ]
    opposite = [(i, (i + 2) % owners) for i in range(owners)]
    swap = [(i, i ^ 1) for i in range(stages)]
    near = lax.ppermute(point_weight, ("sp", "tp"), aside)
    half = lax.dynamic_slice_in_dim(point_weight, core * half_width, half_width, 0)
    half = lax.ppermute(half, "tp", opposite)

    gated = gate(conv_value, conv_gate)
    table = jnp.concatenate([conv_taps, conv_gain[None, :]], axis=0)
    mixed = call(
        conv_kernel, [VMEM] * 4, shape((owners, rows + PACK, width), F32),
        [pltpu.VMEM((width // LANES, block_rows + 2 * HALO, LANES), F32)], 10**9, 16,
    )(gated, low, high, table)
    near, half, _ = lax.optimization_barrier((near, half, mixed))
    swapped = lax.ppermute(near, "sp", swap)
    rest = lax.ppermute(half, "sp", swap)
    mixed = lax.all_to_all(mixed, "tp", split_axis=0, concat_axis=0, tiled=True)

    ids = expert_ids.T
    after, box = call(
        dispatch_kernel, [SMEM] + [VMEM] * 9,
        [shape((rows, features), BF16), shape((experts * PACK, span), BF16)],
        [pltpu.VMEM((owners, rows, width), BF16), pltpu.VMEM((parts * rows, span), BF16)],
        10**9, 32,
    )(jnp.stack([place, core]), mixed, latents, point_weight, near, swapped, half, rest, channel_gain[None, :], ids)

    box = box.reshape(members, PACK, span)
    arrived = lax.all_to_all(box, ("sp", "tp"), split_axis=0, concat_axis=0, tiled=True)
    hidden_width = gate_weight.shape[2]
    answer = call(
        expert_kernel, [VMEM] * 4, shape((members * PACK, span), BF16),
        [
            pltpu.VMEM((parts, members * cap, span), BF16),
            pltpu.VMEM((members * cap, hidden_width), BF16),
            pltpu.VMEM((parts, members * cap, span), BF16),
        ],
        5 * 10**9, 24,
    )(arrived.reshape(members * PACK, span), gate_weight[0], up_weight[0], down_weight[0])
    answer = answer.reshape(members, PACK, span)
    returned = lax.all_to_all(answer, ("sp", "tp"), split_axis=0, concat_axis=0, tiled=True)
    return call(combine_kernel, [VMEM] * 4, shape((rows, features), BF16), [], 10**9, 32)(
        returned.reshape(experts * PACK, span), after, ids, expert_weights.T
    )


def solution(mesh):
    tokens = ("grp", "sp", "tp")
    return jax.shard_map(
        shards,
        mesh=mesh,
        in_specs=(
            P(tokens, None),
            P(("grp", "sp"), "tp"),
            P(("grp", "sp"), "tp"),
            P(None, "tp"),
            P("tp"),
            P("tp", None),
            P(),
            P(tokens, None),
            P(tokens, None),
            P(("sp", "tp"), None, None),
            P(("sp", "tp"), None, None),
            P(("sp", "tp"), None, None),
        ),
        out_specs=P(tokens, None),
        check_vma=False,
    )
```

profile of v0, /device:TPU:33, one launch (start us, length us, event | category | flops | bytes accessed | tf_op | source)
XLA Modules:
  0.0 292.5 jit_solution(17265824988930743544)
XLA Ops:
  0.0 3.7 %collective-permute-start.2 = (bf16[256,2048]{1,0:T(8,128)(2,1)}, bf16[256,2048]{1,0:T(8,128)(2,1)S(1)}, u32[]{:S(2)}, u32[]{:S(2)}) collective-permute-start(bf16[256,2048]{1,0:T(8,128)(2,1)} %own_ref.1), channel_id=1, source_target_pairs={{0,1},{1,2},{2,3},{3,0},{4,7},{5,4},{6,5},{7,6},{8,9},{9,10},{10,1... | collective-permute-start | bytes 3145736 | tf_op jit(solution)/shard_map/ppermute | solution.py:247
  3.7 1.1 constant_dynamic-slice_fusion
  4.8 0.4 collective-permute-start.3
  5.2 0.8 multiply_convert_fusion.1
  6.0 18.4 %collective-permute-start.1 = (bf16[16,256]{1,0:T(8,128)(2,1)S(1)}, bf16[16,256]{1,0:T(8,128)(2,1)S(1)}, u32[]{:S(2)}, u32[]{:S(2)}) collective-permute-start(bf16[16,256]{1,0:T(8,128)(2,1)S(1)} %get-tuple-element.13), channel_id=1, source_target_pairs={{4,0},{8,4},{12,8},{16,12},{20,16},{24,20},{28,24},{32,28},{36,32}... | collective-permute-start | bytes 24584 | tf_op jit(solution)/shard_map/ppermute | solution.py:235
  24.4 2.0 collective-permute-start
  26.4 1.2 multiply_convert_fusion.rows_ref
  27.5 0.8 pad_maximum_fusion.table_ref
  28.3 0.0 copy-start
  28.3 0.0 copy-start.1
  28.3 0.0 copy-start.2
  28.4 0.0 copy-start.3
  28.4 0.0 collective-permute-done.1.high_ref
  28.4 0.0 collective-permute-done.low_ref
  28.4 1.9 shard_map.118
  30.3 0.0 collective-permute-done.3.half_ref
  30.3 0.0 collective-permute-done.2.near_ref
  30.3 12.0 %collective-permute-start.4 = (bf16[256,2048]{1,0:T(8,128)(2,1)S(1)}, bf16[256,2048]{1,0:T(8,128)(2,1)}, u32[]{:S(2)}, u32[]{:S(2)}) collective-permute-start(bf16[256,2048]{1,0:T(8,128)(2,1)S(1)} %collective-permute-done.2.near_ref), channel_id=1, source_target_pairs={{0,4},{4,0},{8,12},{12,8},{16,20},{20,16},{24,28},{28,24},{32,36},... | collective-permute-start | bytes 3145736 | tf_op jit(solution)/shard_map/ppermute | solution.py:258
  42.3 0.0 collective-permute-start.5
  42.3 3.6 %all-to-all-start = ((f32[4,136,256]{2,1,0:T(8,128)}), f32[4,136,256]{2,1,0:T(8,128)S(1)}, u32[]{:S(2)}, u32[]{:S(2)}) async-start(f32[4,136,256]{2,1,0:T(8,128)} %shard_map.118), calls=%async_computation | async-start | bytes 1114112 | tf_op jit(solution)/shard_map/all_to_all | solution.py:260
  45.8 0.1 pad_add_fusion.place_ref
  45.9 9.2 %all-to-all-done.mixed_ref = f32[4,136,256]{2,1,0:T(8,128)S(1)} async-done(((f32[4,136,256]{2,1,0:T(8,128)}), f32[4,136,256]{2,1,0:T(8,128)S(1)}, u32[]{:S(2)}, u32[]{:S(2)}) %all-to-all-start) | async-done | bytes 557088 | tf_op jit(solution)/shard_map/all_to_all | solution.py:260
  55.1 0.0 collective-permute-done.5.rest_ref
  55.2 0.0 collective-permute-done.4.swapped_ref
  55.2 0.0 copy-done
  55.2 0.0 copy-done.1
  55.2 0.0 copy-done.2
  55.2 0.0 copy-done.3
  55.2 0.0 copy-start.5
  55.2 0.0 copy-start.6
  55.2 4.0 %shard_map.119 = (bf16[128,2048]{1,0:T(8,128)(2,1)S(1)}, bf16[1024,1024]{1,0:T(8,128)(2,1)S(1)}) custom-call(s32[2]{0:T(128)S(1)} %pad_add_fusion.place_ref, f32[4,136,256]{2,1,0:T(8,128)S(1)} %all-to-all-done.mixed_ref, bf16[128,2048]{1,0:T(8,128)(2,1)S(1)} %copy-done.1, bf16[256,2048]{1,0:T(8,128)(2,1)S(1)} %copy-done, ...), custom_call_target="tpu_custom_call" | custom-call | flops 1000000000 | bytes 1048576 | tf_op jit(solution)/shard_map/pallas_call | solution.py:263
  59.2 0.0 copy-start.4
  59.2 114.9 %all_to_all.15 = bf16[128,8,1024]{2,1,0:T(8,128)(2,1)S(1)} all-to-all(bf16[128,8,1024]{2,1,0:T(8,128)(2,1)S(1)} %bitcast.13), channel_id=1, replica_groups=mesh['grp'=2,'sp'=32,'tp'=4] {'sp','tp'}, dimensions={0} | all-to-all | bytes 4194304 | tf_op jit(solution)/shard_map/all_to_all | solution.py:271
  174.1 0.0 copy-done.5
  174.1 0.0 copy-done.6
  174.1 0.0 copy-done.4
  174.1 8.3 %shard_map.120 = bf16[1024,1024]{1,0:T(8,128)(2,1)S(1)} custom-call(bf16[1024,1024]{1,0:T(8,128)(2,1)S(1)} %bitcast.15, bf16[2048,768]{1,0:T(8,128)(2,1)S(1)} %bitcast.20, bf16[2048,768]{1,0:T(8,128)(2,1)S(1)} %bitcast.21, bf16[768,2048]{1,0:T(8,128)(2,1)S(1)} %bitcast.22), custom_call_target="tpu_custom_call" | custom-call | flops 5000000000 | bytes 1048576 | tf_op jit(solution)/shard_map/pallas_call | solution.py:273
  182.5 0.0 copy-start.7
  182.5 107.5 %all_to_all.16 = bf16[128,8,1024]{2,1,0:T(8,128)(2,1)S(1)} all-to-all(bf16[128,8,1024]{2,1,0:T(8,128)(2,1)S(1)} %bitcast.16), channel_id=1, replica_groups=mesh['grp'=2,'sp'=32,'tp'=4] {'sp','tp'}, dimensions={0} | all-to-all | bytes 4194304 | tf_op jit(solution)/shard_map/all_to_all | solution.py:283
  290.0 0.0 copy-done.7
  290.0 2.5 shard_map.121
Async XLA Ops:
  0.0 30.3 %collective-permute-start.2 = (bf16[256,2048]{1,0:T(8,128)(2,1)}, bf16[256,2048]{1,0:T(8,128)(2,1)S(1)}, u32[]{:S(2)}, u32[]{:S(2)}) collective-permute-start(bf16[256,2048]{1,0:T(8,128)(2,1)} %own_ref.1), channel_id=1, source_target_pairs={{0,1},{1,2},{2,3},{3,0},{4,7},{5,4},{6,5},{7,6},{8,9},{9,10},{10,1... | collective-permute-start | bytes 3145736 | tf_op jit(solution)/shard_map/ppermute | solution.py:247
  4.8 25.5 %collective-permute-start.3 = (bf16[128,2048]{1,0:T(8,128)(2,1)S(1)}, bf16[128,2048]{1,0:T(8,128)(2,1)}, u32[]{:S(2)}, u32[]{:S(2)}) collective-permute-start(bf16[128,2048]{1,0:T(8,128)(2,1)S(1)} %constant_dynamic-slice_fusion), channel_id=1, source_target_pairs={{0,2},{1,3},{2,0},{3,1},{4,6},{5,7},{6,4},{7,5},{8,10},{9,11},{10,... | collective-permute-start | bytes 1572872 | tf_op jit(solution)/shard_map/ppermute | solution.py:249
  6.0 22.4 %collective-permute-start.1 = (bf16[16,256]{1,0:T(8,128)(2,1)S(1)}, bf16[16,256]{1,0:T(8,128)(2,1)S(1)}, u32[]{:S(2)}, u32[]{:S(2)}) collective-permute-start(bf16[16,256]{1,0:T(8,128)(2,1)S(1)} %get-tuple-element.13), channel_id=1, source_target_pairs={{4,0},{8,4},{12,8},{16,12},{20,16},{24,20},{28,24},{32,28},{36,32}... | collective-permute-start | bytes 24584 | tf_op jit(solution)/shard_map/ppermute | solution.py:235
  24.4 4.0 %collective-permute-start = (bf16[16,256]{1,0:T(8,128)(2,1)S(1)}, bf16[16,256]{1,0:T(8,128)(2,1)S(1)}, u32[]{:S(2)}, u32[]{:S(2)}) collective-permute-start(bf16[16,256]{1,0:T(8,128)(2,1)S(1)} %get-tuple-element.14), channel_id=1, source_target_pairs={{0,4},{4,8},{8,12},{12,16},{16,20},{20,24},{24,28},{28,32},{32,36}... | collective-permute-start | bytes 24584 | tf_op jit(solution)/shard_map/ppermute | solution.py:234
  28.3 26.8 %copy-start = (bf16[256,2048]{1,0:T(8,128)(2,1)S(1)}, bf16[256,2048]{1,0:T(8,128)(2,1)}, u32[]{:S(2)}) copy-start(bf16[256,2048]{1,0:T(8,128)(2,1)} %own_ref.1) | copy-start | bytes 3145732
  28.3 26.8 %copy-start.1 = (bf16[128,2048]{1,0:T(8,128)(2,1)S(1)}, bf16[128,2048]{1,0:T(8,128)(2,1)}, u32[]{:S(2)}) copy-start(bf16[128,2048]{1,0:T(8,128)(2,1)} %latents_ref.1) | copy-start | bytes 1572868
  28.3 26.8 %copy-start.2 = (f32[2048]{0:T(1024)S(1)}, f32[2048]{0:T(1024)}, u32[]{:S(2)}) copy-start(f32[2048]{0:T(1024)} %param.18) | copy-start | bytes 24580
  28.4 26.8 %copy-start.3 = (s32[128,2]{0,1:T(2,128)S(1)}, s32[128,2]{0,1:T(2,128)}, u32[]{:S(2)}) copy-start(s32[128,2]{0,1:T(2,128)} %param.19) | copy-start | bytes 3076
  30.3 24.9 %collective-permute-start.4 = (bf16[256,2048]{1,0:T(8,128)(2,1)S(1)}, bf16[256,2048]{1,0:T(8,128)(2,1)}, u32[]{:S(2)}, u32[]{:S(2)}) collective-permute-start(bf16[256,2048]{1,0:T(8,128)(2,1)S(1)} %collective-permute-done.2.near_ref), channel_id=1, source_target_pairs={{0,4},{4,0},{8,12},{12,8},{16,20},{20,16},{24,28},{28,24},{32,36},... | collective-permute-start | bytes 3145736 | tf_op jit(solution)/shard_map/ppermute | solution.py:258
  42.3 12.9 %collective-permute-start.5 = (bf16[128,2048]{1,0:T(8,128)(2,1)}, bf16[128,2048]{1,0:T(8,128)(2,1)}, u32[]{:S(2)}, u32[]{:S(2)}) collective-permute-start(bf16[128,2048]{1,0:T(8,128)(2,1)} %collective-permute-done.3.half_ref), channel_id=1, source_target_pairs={{0,4},{4,0},{8,12},{12,8},{16,20},{20,16},{24,28},{28,24},{32,36},... | collective-permute-start | bytes 1572872 | tf_op jit(solution)/shard_map/ppermute | solution.py:259
  42.3 12.9 %all-to-all-start = ((f32[4,136,256]{2,1,0:T(8,128)}), f32[4,136,256]{2,1,0:T(8,128)S(1)}, u32[]{:S(2)}, u32[]{:S(2)}) async-start(f32[4,136,256]{2,1,0:T(8,128)} %shard_map.118), calls=%async_computation | async-start | bytes 1114112 | tf_op jit(solution)/shard_map/all_to_all | solution.py:260
  55.2 118.9 %copy-start.5 = (bf16[1,2048,768]{2,1,0:T(8,128)(2,1)S(1)}, bf16[1,2048,768]{2,1,0:T(8,128)(2,1)}, u32[]{:S(2)}) copy-start(bf16[1,2048,768]{2,1,0:T(8,128)(2,1)} %param.22) | copy-start | bytes 9437188
  55.2 118.9 %copy-start.6 = (bf16[1,768,2048]{2,1,0:T(8,128)(2,1)S(1)}, bf16[1,768,2048]{2,1,0:T(8,128)(2,1)}, u32[]{:S(2)}) copy-start(bf16[1,768,2048]{2,1,0:T(8,128)(2,1)} %param.23) | copy-start | bytes 9437188
  59.2 114.9 %copy-start.4 = (bf16[1,2048,768]{2,1,0:T(8,128)(2,1)S(1)}, bf16[1,2048,768]{2,1,0:T(8,128)(2,1)}, u32[]{:S(2)}) copy-start(bf16[1,2048,768]{2,1,0:T(8,128)(2,1)} %param.21) | copy-start | bytes 9437188
  182.5 107.5 %copy-start.7 = (f32[128,2]{0,1:T(2,128)S(1)}, f32[128,2]{0,1:T(2,128)}, u32[]{:S(2)}) copy-start(f32[128,2]{0,1:T(2,128)} %param.20) | copy-start | bytes 3076
where the time goes:
time: 293 us
  blocking collectives  222 us (76%)
  starting transfers between devices  40 us (14%)
  Pallas kernels  16.8 us (6%)
  waiting for transfers between devices  9.25 us (3%)
    all_to_all x1, blocking collectives, shards(): lax.all_to_all(box, ('sp', 'tp'), split_axis=0, concat_axis=0, tiled=True)  115 us
    all_to_all x1, blocking collectives, shards(): lax.all_to_all(answer, ('sp', 'tp'), split_axis=0, concat_axis=0, tiled=T...  108 us
    ppermute x1, starting transfers between devices, shards(): high = lax.ppermute(gate(conv_value[:HALO], conv_gate[:HALO]), 'sp', behind)  18.4 us
    ppermute x1, starting transfers between devices, shards(): swapped = lax.ppermute(near, 'sp', swap)  12 us
    all_to_all x1, waiting for transfers between devices, shards(): mixed = lax.all_to_all(mixed, 'tp', split_axis=0, concat_axis=0, tiled=True)  9.24 us
    pallas_call x1, Pallas kernels, shards(): call(expert_kernel, [VMEM] * 4, shape((members * PACK, span), BF16), [plt...  8.35 us
  transfers between devices with their start and end apart: 7, of which 1 were waited for; matrix products, arithmetic and copies ran while one was open for 1% of the time, Pallas kernels for 1%

commit v1 on v0

--- a/solution.py
+++ b/solution.py
@@ -150,7 +150,7 @@
         hidden_ref[:, cols] = (gated * jax.nn.sigmoid(gated) * upped).astype(BF16)
         return carry
 
-    lax.fori_loop(0, hidden_width // tile, inner, 0)
+    lax.fori_loop(0, hidden_width // tile, inner, 0, unroll=True)
     for part in range(parts):
 
         def outer(n, carry, part=part):
@@ -159,7 +159,7 @@
             y_ref[part, :, cols] = dot(hidden_ref[...], weights).astype(BF16)
             return carry
 
-        lax.fori_loop(0, span // tile, outer, 0)
+        lax.fori_loop(0, span // tile, outer, 0, unroll=True)
     backward = shuffle_matrix(block, parts, True)
     for i in range(in_ref.shape[0] // block):
         stacked = jnp.concatenate(
@@ -242,11 +242,8 @@
         for stage in range(stages)
         for i in range(owners)
     ]
-    opposite = [(i, (i + 2) % owners) for i in range(owners)]
     swap = [(i, i ^ 1) for i in range(stages)]
     near = lax.ppermute(point_weight, ("sp", "tp"), aside)
-    half = lax.dynamic_slice_in_dim(point_weight, core * half_width, half_width, 0)
-    half = lax.ppermute(half, "tp", opposite)
 
     gated = gate(conv_value, conv_gate)
     table = jnp.concatenate([conv_taps, conv_gain[None, :]], axis=0)
@@ -254,7 +251,9 @@
         conv_kernel, [VMEM] * 4, shape((owners, rows + PACK, width), F32),
         [pltpu.VMEM((width // LANES, block_rows + 2 * HALO, LANES), F32)], 10**9, 16,
     )(gated, low, high, table)
-    near, half, _ = lax.optimization_barrier((near, half, mixed))
+    near, _ = lax.optimization_barrier((near, mixed))
+    half = lax.dynamic_slice_in_dim(near, core * half_width, half_width, 0)
+    half = lax.ppermute(half, ("sp", "tp"), aside)
     swapped = lax.ppermute(near, "sp", swap)
     rest = lax.ppermute(half, "sp", swap)
     mixed = lax.all_to_all(mixed, "tp", split_axis=0, concat_axis=0, tiled=True)

time: 293 us -> 289 us (0.986)
  blocking collectives: 222 us -> 215 us
  starting transfers between devices: 40 us -> 44.8 us
    ppermute x1, starting transfers between devices: 0.01 us -> 9.02 us  [shards(): rest = lax.ppermute(half, 'sp', swap)]
    all_to_all x1, blocking collectives: 115 us -> 107 us  [shards(): lax.all_to_all(box, ('sp', 'tp'), split_axis=0, concat_axis=0, tiled=True)]
    ppermute x1, starting transfers between devices: 12 us -> 4.8 us  [shards(): swapped = lax.ppermute(near, 'sp', swap)]
  transfers between devices with their start and end apart: 7 -> 7, of which waited for: 1 -> 2; matrix products, arithmetic and copies ran while one was open for 1% -> 1% of each run, Pallas kernels for 1% -> 1%
where the time goes in v1:
time: 289 us; the launch traced here: 288 us
  blocking collectives  215 us (74%)
  starting transfers between devices  44.8 us (16%)
  Pallas kernels  14.6 us (5%)
  waiting for transfers between devices  11.1 us (4%)
    all_to_all x1, blocking collectives, shards(): lax.all_to_all(answer, ('sp', 'tp'), split_axis=0, concat_axis=0, tiled=T...  107 us
    all_to_all x1, blocking collectives, shards(): lax.all_to_all(box, ('sp', 'tp'), split_axis=0, concat_axis=0, tiled=True)  107 us
    ppermute x1, starting transfers between devices, shards(): high = lax.ppermute(gate(conv_value[:HALO], conv_gate[:HALO]), 'sp', behind)  18.7 us
    all_to_all x1, waiting for transfers between devices, shards(): mixed = lax.all_to_all(mixed, 'tp', split_axis=0, concat_axis=0, tiled=True)  9.74 us
    ppermute x1, starting transfers between devices, shards(): rest = lax.ppermute(half, 'sp', swap)  9.02 us
    pallas_call x1, Pallas kernels, shards(): call(expert_kernel, [VMEM] * 4, shape((members * PACK, span), BF16), [plt...  6.15 us
  transfers between devices with their start and end apart: 7, of which 2 were waited for; matrix products, arithmetic and copies ran while one was open for 1% of the time, Pallas kernels for 1%

profile of v1, /device:TPU:33, one launch (start us, length us, event | category | flops | bytes accessed | tf_op | source)
XLA Modules:
  0.0 288.2 jit_solution(14545683493885881354)
XLA Ops:
  0.0 3.7 %collective-permute-start.2 = (bf16[256,2048]{1,0:T(8,128)(2,1)}, bf16[256,2048]{1,0:T(8,128)(2,1)S(1)}, u32[]{:S(2)}, u32[]{:S(2)}) collective-permute-start(bf16[256,2048]{1,0:T(8,128)(2,1)} %own_ref.1), channel_id=1, source_target_pairs={{0,1},{1,2},{2,3},{3,0},{4,7},{5,4},{6,5},{7,6},{8,9},{9,10},{10,1... | collective-permute-start | bytes 3145736 | tf_op jit(solution)/shard_map/ppermute | solution.py:246
  3.7 0.8 multiply_convert_fusion.1
  4.5 18.7 %collective-permute-start.1 = (bf16[16,256]{1,0:T(8,128)(2,1)S(1)}, bf16[16,256]{1,0:T(8,128)(2,1)S(1)}, u32[]{:S(2)}, u32[]{:S(2)}) collective-permute-start(bf16[16,256]{1,0:T(8,128)(2,1)S(1)} %get-tuple-element.11), channel_id=1, source_target_pairs={{4,0},{8,4},{12,8},{16,12},{20,16},{24,20},{28,24},{32,28},{36,32}... | collective-permute-start | bytes 24584 | tf_op jit(solution)/shard_map/ppermute | solution.py:235
  23.1 2.0 collective-permute-start
  25.1 1.2 multiply_convert_fusion.rows_ref
  26.3 0.8 pad_maximum_fusion.table_ref
  27.1 0.0 copy-start
  27.1 0.0 copy-start.1
  27.1 0.0 copy-start.2
  27.1 0.0 copy-start.3
  27.1 0.0 collective-permute-done.1.high_ref
  27.1 0.0 collective-permute-done.low_ref
  27.1 1.9 shard_map.118
  29.0 0.0 collective-permute-done.2.near_ref
  29.1 3.1 %collective-permute-start.4 = (bf16[128,2048]{1,0:T(8,128)(2,1)S(1)}, bf16[128,2048]{1,0:T(8,128)(2,1)}, u32[]{:S(2)}, u32[]{:S(2)}) collective-permute-start(bf16[128,2048]{1,0:T(8,128)(2,1)S(1)} %constant_dynamic-slice_fusion), channel_id=1, source_target_pairs={{0,1},{1,2},{2,3},{3,0},{4,7},{5,4},{6,5},{7,6},{8,9},{9,10},{10,1... | collective-permute-start | bytes 1572872 | tf_op jit(solution)/shard_map/ppermute | solution.py:256
  32.1 4.8 %collective-permute-start.3 = (bf16[256,2048]{1,0:T(8,128)(2,1)S(1)}, bf16[256,2048]{1,0:T(8,128)(2,1)}, u32[]{:S(2)}, u32[]{:S(2)}) collective-permute-start(bf16[256,2048]{1,0:T(8,128)(2,1)S(1)} %collective-permute-done.2.near_ref), channel_id=1, source_target_pairs={{0,4},{4,0},{8,12},{12,8},{16,20},{20,16},{24,28},{28,24},{32,36},... | collective-permute-start | bytes 3145736 | tf_op jit(solution)/shard_map/ppermute | solution.py:257
  36.9 1.3 collective-permute-done.4.half_ref
  38.3 9.0 %collective-permute-start.5 = (bf16[128,2048]{1,0:T(8,128)(2,1)}, bf16[128,2048]{1,0:T(8,128)(2,1)}, u32[]{:S(2)}, u32[]{:S(2)}) collective-permute-start(bf16[128,2048]{1,0:T(8,128)(2,1)} %collective-permute-done.4.half_ref), channel_id=1, source_target_pairs={{0,4},{4,0},{8,12},{12,8},{16,20},{20,16},{24,28},{28,24},{32,36},... | collective-permute-start | bytes 1572872 | tf_op jit(solution)/shard_map/ppermute | solution.py:258
  47.3 3.6 %all-to-all-start = ((f32[4,136,256]{2,1,0:T(8,128)}), f32[4,136,256]{2,1,0:T(8,128)S(1)}, u32[]{:S(2)}, u32[]{:S(2)}) async-start(f32[4,136,256]{2,1,0:T(8,128)} %shard_map.118), calls=%async_computation | async-start | bytes 1114112 | tf_op jit(solution)/shard_map/all_to_all | solution.py:259
  50.9 0.1 pad_add_fusion.place_ref
  50.9 9.7 %all-to-all-done.mixed_ref = f32[4,136,256]{2,1,0:T(8,128)S(1)} async-done(((f32[4,136,256]{2,1,0:T(8,128)}), f32[4,136,256]{2,1,0:T(8,128)S(1)}, u32[]{:S(2)}, u32[]{:S(2)}) %all-to-all-start) | async-done | bytes 557088 | tf_op jit(solution)/shard_map/all_to_all | solution.py:259
  60.7 0.0 collective-permute-done.5.rest_ref
  60.7 0.0 collective-permute-done.3.swapped_ref
  60.7 0.0 copy-done
  60.7 0.0 copy-done.1
  60.7 0.0 copy-done.2
  60.7 0.0 copy-done.3
  60.7 0.0 copy-start.5
  60.7 0.0 copy-start.6
  60.8 4.0 %shard_map.119 = (bf16[128,2048]{1,0:T(8,128)(2,1)S(1)}, bf16[1024,1024]{1,0:T(8,128)(2,1)S(1)}) custom-call(s32[2]{0:T(128)S(1)} %pad_add_fusion.place_ref, f32[4,136,256]{2,1,0:T(8,128)S(1)} %all-to-all-done.mixed_ref, bf16[128,2048]{1,0:T(8,128)(2,1)S(1)} %copy-done.1, bf16[256,2048]{1,0:T(8,128)(2,1)S(1)} %copy-done, ...), custom_call_target="tpu_custom_call" | custom-call | flops 1000000000 | bytes 1048576 | tf_op jit(solution)/shard_map/pallas_call | solution.py:262
  64.8 0.0 copy-start.4
  64.8 107.3 %all_to_all.15 = bf16[128,8,1024]{2,1,0:T(8,128)(2,1)S(1)} all-to-all(bf16[128,8,1024]{2,1,0:T(8,128)(2,1)S(1)} %bitcast.13), channel_id=1, replica_groups=mesh['grp'=2,'sp'=32,'tp'=4] {'sp','tp'}, dimensions={0} | all-to-all | bytes 4194304 | tf_op jit(solution)/shard_map/all_to_all | solution.py:270
  172.0 0.0 copy-done.5
  172.0 0.0 copy-done.6
  172.1 0.0 copy-done.4
  172.1 6.2 %shard_map.120 = bf16[1024,1024]{1,0:T(8,128)(2,1)S(1)} custom-call(bf16[1024,1024]{1,0:T(8,128)(2,1)S(1)} %bitcast.15, bf16[2048,768]{1,0:T(8,128)(2,1)S(1)} %bitcast.20, bf16[2048,768]{1,0:T(8,128)(2,1)S(1)} %bitcast.21, bf16[768,2048]{1,0:T(8,128)(2,1)S(1)} %bitcast.22), custom_call_target="tpu_custom_call" | custom-call | flops 5000000000 | bytes 1048576 | tf_op jit(solution)/shard_map/pallas_call | solution.py:272
  178.2 0.0 copy-start.7
  178.2 107.5 %all_to_all.16 = bf16[128,8,1024]{2,1,0:T(8,128)(2,1)S(1)} all-to-all(bf16[128,8,1024]{2,1,0:T(8,128)(2,1)S(1)} %bitcast.16), channel_id=1, replica_groups=mesh['grp'=2,'sp'=32,'tp'=4] {'sp','tp'}, dimensions={0} | all-to-all | bytes 4194304 | tf_op jit(solution)/shard_map/all_to_all | solution.py:282
  285.7 0.0 copy-done.7
  285.7 2.5 shard_map.121
  (1 shorter events, 0.0 us)
Async XLA Ops:
  0.0 29.0 %collective-permute-start.2 = (bf16[256,2048]{1,0:T(8,128)(2,1)}, bf16[256,2048]{1,0:T(8,128)(2,1)S(1)}, u32[]{:S(2)}, u32[]{:S(2)}) collective-permute-start(bf16[256,2048]{1,0:T(8,128)(2,1)} %own_ref.1), channel_id=1, source_target_pairs={{0,1},{1,2},{2,3},{3,0},{4,7},{5,4},{6,5},{7,6},{8,9},{9,10},{10,1... | collective-permute-start | bytes 3145736 | tf_op jit(solution)/shard_map/ppermute | solution.py:246
  4.5 22.6 %collective-permute-start.1 = (bf16[16,256]{1,0:T(8,128)(2,1)S(1)}, bf16[16,256]{1,0:T(8,128)(2,1)S(1)}, u32[]{:S(2)}, u32[]{:S(2)}) collective-permute-start(bf16[16,256]{1,0:T(8,128)(2,1)S(1)} %get-tuple-element.11), channel_id=1, source_target_pairs={{4,0},{8,4},{12,8},{16,12},{20,16},{24,20},{28,24},{32,28},{36,32}... | collective-permute-start | bytes 24584 | tf_op jit(solution)/shard_map/ppermute | solution.py:235
  23.1 4.0 %collective-permute-start = (bf16[16,256]{1,0:T(8,128)(2,1)S(1)}, bf16[16,256]{1,0:T(8,128)(2,1)S(1)}, u32[]{:S(2)}, u32[]{:S(2)}) collective-permute-start(bf16[16,256]{1,0:T(8,128)(2,1)S(1)} %get-tuple-element.12), channel_id=1, source_target_pairs={{0,4},{4,8},{8,12},{12,16},{16,20},{20,24},{24,28},{28,32},{32,36}... | collective-permute-start | bytes 24584 | tf_op jit(solution)/shard_map/ppermute | solution.py:234
  27.1 33.6 %copy-start = (bf16[256,2048]{1,0:T(8,128)(2,1)S(1)}, bf16[256,2048]{1,0:T(8,128)(2,1)}, u32[]{:S(2)}) copy-start(bf16[256,2048]{1,0:T(8,128)(2,1)} %own_ref.1) | copy-start | bytes 3145732
  27.1 33.6 %copy-start.1 = (bf16[128,2048]{1,0:T(8,128)(2,1)S(1)}, bf16[128,2048]{1,0:T(8,128)(2,1)}, u32[]{:S(2)}) copy-start(bf16[128,2048]{1,0:T(8,128)(2,1)} %latents_ref.1) | copy-start | bytes 1572868
  27.1 33.6 %copy-start.2 = (f32[2048]{0:T(1024)S(1)}, f32[2048]{0:T(1024)}, u32[]{:S(2)}) copy-start(f32[2048]{0:T(1024)} %param.18) | copy-start | bytes 24580
  27.1 33.6 %copy-start.3 = (s32[128,2]{0,1:T(2,128)S(1)}, s32[128,2]{0,1:T(2,128)}, u32[]{:S(2)}) copy-start(s32[128,2]{0,1:T(2,128)} %param.19) | copy-start | bytes 3076
  29.1 9.2 %collective-permute-start.4 = (bf16[128,2048]{1,0:T(8,128)(2,1)S(1)}, bf16[128,2048]{1,0:T(8,128)(2,1)}, u32[]{:S(2)}, u32[]{:S(2)}) collective-permute-start(bf16[128,2048]{1,0:T(8,128)(2,1)S(1)} %constant_dynamic-slice_fusion), channel_id=1, source_target_pairs={{0,1},{1,2},{2,3},{3,0},{4,7},{5,4},{6,5},{7,6},{8,9},{9,10},{10,1... | collective-permute-start | bytes 1572872 | tf_op jit(solution)/shard_map/ppermute | solution.py:256
  32.1 28.6 %collective-permute-start.3 = (bf16[256,2048]{1,0:T(8,128)(2,1)S(1)}, bf16[256,2048]{1,0:T(8,128)(2,1)}, u32[]{:S(2)}, u32[]{:S(2)}) collective-permute-start(bf16[256,2048]{1,0:T(8,128)(2,1)S(1)} %collective-permute-done.2.near_ref), channel_id=1, source_target_pairs={{0,4},{4,0},{8,12},{12,8},{16,20},{20,16},{24,28},{28,24},{32,36},... | collective-permute-start | bytes 3145736 | tf_op jit(solution)/shard_map/ppermute | solution.py:257
  38.3 22.4 %collective-permute-start.5 = (bf16[128,2048]{1,0:T(8,128)(2,1)}, bf16[128,2048]{1,0:T(8,128)(2,1)}, u32[]{:S(2)}, u32[]{:S(2)}) collective-permute-start(bf16[128,2048]{1,0:T(8,128)(2,1)} %collective-permute-done.4.half_ref), channel_id=1, source_target_pairs={{0,4},{4,0},{8,12},{12,8},{16,20},{20,16},{24,28},{28,24},{32,36},... | collective-permute-start | bytes 1572872 | tf_op jit(solution)/shard_map/ppermute | solution.py:258
  47.3 13.4 %all-to-all-start = ((f32[4,136,256]{2,1,0:T(8,128)}), f32[4,136,256]{2,1,0:T(8,128)S(1)}, u32[]{:S(2)}, u32[]{:S(2)}) async-start(f32[4,136,256]{2,1,0:T(8,128)} %shard_map.118), calls=%async_computation | async-start | bytes 1114112 | tf_op jit(solution)/shard_map/all_to_all | solution.py:259
  60.7 111.3 %copy-start.5 = (bf16[1,2048,768]{2,1,0:T(8,128)(2,1)S(1)}, bf16[1,2048,768]{2,1,0:T(8,128)(2,1)}, u32[]{:S(2)}) copy-start(bf16[1,2048,768]{2,1,0:T(8,128)(2,1)} %param.22) | copy-start | bytes 9437188
  60.7 111.3 %copy-start.6 = (bf16[1,768,2048]{2,1,0:T(8,128)(2,1)S(1)}, bf16[1,768,2048]{2,1,0:T(8,128)(2,1)}, u32[]{:S(2)}) copy-start(bf16[1,768,2048]{2,1,0:T(8,128)(2,1)} %param.23) | copy-start | bytes 9437188
  64.8 107.3 %copy-start.4 = (bf16[1,2048,768]{2,1,0:T(8,128)(2,1)S(1)}, bf16[1,2048,768]{2,1,0:T(8,128)(2,1)}, u32[]{:S(2)}) copy-start(bf16[1,2048,768]{2,1,0:T(8,128)(2,1)} %param.21) | copy-start | bytes 9437188
  178.2 107.5 %copy-start.7 = (f32[128,2]{0,1:T(2,128)S(1)}, f32[128,2]{0,1:T(2,128)}, u32[]{:S(2)}) copy-start(f32[128,2]{0,1:T(2,128)} %param.20) | copy-start | bytes 3076

commit v2 on v1

--- a/solution.py
+++ b/solution.py
@@ -11,6 +11,7 @@
 HALO = 16
 LANES = 128
 PACK = 8
+EXTRA = 16
 
 
 def dot(a, b):
@@ -25,10 +26,22 @@
     return (value.astype(F32) * jax.nn.sigmoid(gating.astype(F32))).astype(BF16)
 
 
-def conv_kernel(rows_ref, low_ref, high_ref, table_ref, out_ref, pad_ref):
+def terms(value):
+    high = value.astype(BF16)
+    rest = value - high.astype(F32)
+    middle = rest.astype(BF16)
+    return high, middle, (rest - middle.astype(F32)).astype(BF16)
+
+
+def joined(block_ref, j, first):
+    rows = [block_ref[j, first + k : first + k + 1, :].astype(F32) for k in range(3)]
+    return rows[0] + rows[1] + rows[2]
+
+
+def conv_kernel(rows_ref, low_ref, high_ref, table_ref, out_ref, pad_ref, sum_ref):
     taps, width = table_ref.shape[0] - 1, table_ref.shape[1]
     rows = rows_ref.shape[0]
-    owners, owner_rows = out_ref.shape[0], out_ref.shape[1] - PACK
+    owners, owner_rows = out_ref.shape[0], out_ref.shape[1] - EXTRA
     step = 64
     parts = [slice(first, first + LANES) for first in range(0, width, LANES)]
     for part, lanes in enumerate(parts):
@@ -41,10 +54,16 @@
             for tap in range(taps):
                 first = start + HALO - taps // 2 + tap
                 total = total + table_ref[tap : tap + 1, lanes] * pad_ref[part, first : first + step]
-            owner, row = divmod(start, owner_rows)
-            out_ref[owner, row : row + step, lanes] = total
+            sum_ref[start : start + step, lanes] = total
+    gains = terms(table_ref[taps:, :])
+    spare = jnp.zeros((EXTRA - 6, width), BF16)
     for owner in range(owners):
-        out_ref[owner, owner_rows:, :] = jnp.broadcast_to(table_ref[taps:, :], (PACK, width))
+        block = sum_ref[owner * owner_rows : (owner + 1) * owner_rows]
+        mean = jnp.sum(block, axis=1, keepdims=True) / width
+        out_ref[owner, :owner_rows] = (block - mean).astype(BF16)
+        across = jnp.transpose(jnp.broadcast_to(mean, (owner_rows, owner_rows)))[:1]
+        across = jnp.concatenate([across, jnp.zeros((1, width - owner_rows), F32)], axis=1)
+        out_ref[owner, owner_rows:] = jnp.concatenate([*gains, *terms(across), spare], axis=0)
 
 
 def slots(ids_ref, experts):
@@ -58,22 +77,61 @@
     return jnp.where(chosen > 0, earlier + 1.0, 0.0)
 
 
-def dispatch_kernel(
-    place_ref, mixed_ref, latents_ref, own_ref, near_ref, swapped_ref, half_ref, rest_ref, gain_ref, ids_ref, after_ref, box_ref, act_ref, x_ref,
-):
+def routing_kernel(ids_ref, weights_ref, pick_ref, factor_ref):
+    rows = ids_ref.shape[1]
+    size = pick_ref.shape[0]
+    parts = pick_ref.shape[1] // rows
+    cap = PACK // parts
+    experts = size // PACK
+    slot = slots(ids_ref, experts)
+    expert = iota((experts, rows), 0)
+    weight = jnp.zeros((experts, rows), F32)
+    for k in range(ids_ref.shape[0]):
+        weight = jnp.where(ids_ref[k : k + 1, :] == expert, weights_ref[k : k + 1, :], weight)
+    weight = jnp.transpose(weight)
+    coarse = weight.astype(BF16)
+    fine = (weight - coarse.astype(F32)).astype(BF16)
+    across = jnp.transpose(slot).astype(BF16)
+    slot = slot.astype(BF16)
+    block = 2 * LANES
+    for start in range(0, size, block):
+        row = iota((block, experts), 0) + start
+        spread = ((row >> 3) == iota((block, experts), 1)).astype(F32).astype(BF16)
+        wanted = dot(spread, slot)
+        row = iota((block, rows), 0)
+        hit = wanted == ((row & (cap - 1)) + 1).astype(F32)
+        for part in range(parts):
+            here = hit & (((row & (PACK - 1)) // cap) == part)
+            pick_ref[start : start + block, part * rows : (part + 1) * rows] = here.astype(F32).astype(BF16)
+    spread = (iota((experts, size), 0) == (iota((experts, size), 1) >> 3)).astype(F32).astype(BF16)
+    column = iota((rows, size), 1)
+    hit = dot(across, spread) == ((column & (cap - 1)) + 1).astype(F32)
+    coarse, fine = dot(coarse, spread), dot(fine, spread)
+    for part in range(parts):
+        here = hit & (((column & (PACK - 1)) // cap) == part)
+        for k, value in enumerate((coarse, fine)):
+            first = (2 * part + k) * rows
+            factor_ref[first : first + rows] = jnp.where(here, value, 0.0).astype(BF16)
+
+
+def partial_kernel(place_ref, mixed_ref, own_ref, near_ref, swapped_ref, half_ref, out_ref, rest_ref, value_ref, act_ref):
     owners, _, width = mixed_ref.shape
-    rows, features = latents_ref.shape
+    rows, features = out_ref.shape
     half_width = width // 2
     total = jnp.zeros((rows, 1), F32)
+    for j in range(owners):
+        across = joined(mixed_ref, j, rows + 3)[:, :rows]
+        mean = jnp.transpose(jnp.broadcast_to(across, (rows, rows)))[:, :1]
+        value_ref[j] = mixed_ref[j, :rows, :].astype(F32) + mean
+        total = total + jnp.sum(value_ref[j], axis=1, keepdims=True)
+    center = total / (owners * width)
     squares = jnp.zeros((rows, 1), F32)
     for j in range(owners):
-        block = mixed_ref[j, :rows, :]
-        total = total + jnp.sum(block, axis=1, keepdims=True)
-        squares = squares + jnp.sum(block * block, axis=1, keepdims=True)
-    center = total / (owners * width)
-    scale = lax.rsqrt(squares / (owners * width) - center * center + 0.05)
+        value = value_ref[j] - center
+        squares = squares + jnp.sum(value * value, axis=1, keepdims=True)
+    scale = lax.rsqrt(squares / (owners * width) + 0.05)
     for j in range(owners):
-        value = (mixed_ref[j, :rows, :] - center) * scale * mixed_ref[j, rows : rows + 1, :]
+        value = (value_ref[j] - center) * scale * joined(mixed_ref, j, rows)
         act_ref[j] = (value * jax.nn.sigmoid(value)).astype(BF16)
     place, core = place_ref[0], place_ref[1]
     before = lax.rem(place + owners - 1 + 2 * core, owners)
@@ -81,41 +139,39 @@
     across = act_ref[lax.rem(place + 2, owners)]
     lower, upper = across[:, :half_width], across[:, half_width:]
     first = jnp.where(core == 0, lower, upper)
-    second = jnp.where(core == 0, upper, lower)
+    rest_ref[...] = jnp.where(core == 0, upper, lower)
     step = 512
-    squares = jnp.zeros((rows, 1), F32)
     for start in range(0, features, step):
         cols = slice(start, start + step)
         branch = dot(act_ref[place], own_ref[:, cols])
         branch = branch + dot(act_ref[before], near_ref[:, cols])
         branch = branch + dot(act_ref[beyond], swapped_ref[:, cols])
-        branch = branch + dot(first, half_ref[:, cols]) + dot(second, rest_ref[:, cols])
+        out_ref[:, cols] = branch + dot(first, half_ref[:, cols])
+
+
+def dispatch_kernel(
+    latents_ref, partial_ref, act_ref, rest_ref, gain_ref, pick_ref, after_ref, box_ref, x_ref
+):
+    rows, features = latents_ref.shape
+    step = 512
+    squares = jnp.zeros((rows, 1), F32)
+    for start in range(0, features, step):
+        cols = slice(start, start + step)
+        branch = partial_ref[:, cols] + dot(act_ref[...], rest_ref[:, cols])
         after = (latents_ref[:, cols].astype(F32) + branch).astype(BF16)
         after_ref[:, cols] = after
         after = after.astype(F32)
         squares = squares + jnp.sum(after * after, axis=1, keepdims=True)
     scale = lax.rsqrt(squares / features + 0.01)
-    parts, cap = x_ref.shape[0] // rows, PACK * rows // x_ref.shape[0]
+    parts = x_ref.shape[0] // rows
     span = features // parts
     for part in range(parts):
         cols = slice(part * span, (part + 1) * span)
         value = after_ref[:, cols].astype(F32) * scale * gain_ref[:, cols]
         x_ref[part * rows : (part + 1) * rows] = value.astype(BF16)
-    experts = box_ref.shape[0] // PACK
-    slot = slots(ids_ref, experts).astype(BF16)
     block = 2 * LANES
     for start in range(0, box_ref.shape[0], block):
-        row = iota((block, experts), 0) + start
-        spread = ((row >> 3) == iota((block, experts), 1)).astype(F32).astype(BF16)
-        wanted = dot(spread, slot)
-        row = iota((block, rows), 0)
-        hit = wanted == ((row & (cap - 1)) + 1).astype(F32)
-        picks = [
-            (hit & (((row & (PACK - 1)) // cap) == part)).astype(F32).astype(BF16)
-            for part in range(parts)
-        ]
-        pick = jnp.concatenate(picks, axis=1)
-        box_ref[start : start + block] = dot(pick, x_ref[...]).astype(BF16)
+        box_ref[start : start + block] = dot(pick_ref[start : start + block], x_ref[...]).astype(BF16)
 
 
 def shuffle_matrix(size, parts, inverse):
@@ -168,31 +224,11 @@
         out_ref[i * block : (i + 1) * block] = dot(backward, stacked).astype(BF16)
 
 
-def combine_kernel(in_ref, after_ref, ids_ref, weights_ref, out_ref):
+def combine_kernel(in_ref, after_ref, factor_ref, out_ref):
     rows, features = after_ref.shape
-    size, span = in_ref.shape
-    parts = features // span
-    cap = PACK // parts
-    experts = size // PACK
-    slot = jnp.transpose(slots(ids_ref, experts)).astype(BF16)
-    expert = iota((experts, rows), 0)
-    weight = jnp.zeros((experts, rows), F32)
-    for k in range(ids_ref.shape[0]):
-        weight = jnp.where(ids_ref[k : k + 1, :] == expert, weights_ref[k : k + 1, :], weight)
-    weight = jnp.transpose(weight)
-    coarse = weight.astype(BF16)
-    fine = (weight - coarse.astype(F32)).astype(BF16)
-    spread = (iota((experts, size), 0) == (iota((experts, size), 1) >> 3)).astype(F32).astype(BF16)
-    column = iota((rows, size), 1)
-    hit = dot(slot, spread) == ((column & (cap - 1)) + 1).astype(F32)
-    coarse = jnp.where(hit, dot(coarse, spread), 0.0)
-    fine = jnp.where(hit, dot(fine, spread), 0.0)
-    for part in range(parts):
-        here = ((column & (PACK - 1)) // cap) == part
-        factors = jnp.concatenate(
-            [jnp.where(here, coarse, 0.0).astype(BF16), jnp.where(here, fine, 0.0).astype(BF16)], axis=0
-        )
-        sums = dot(factors, in_ref[...])
+    span = in_ref.shape[1]
+    for part in range(features // span):
+        sums = dot(factor_ref[2 * part * rows : 2 * (part + 1) * rows], in_ref[...])
         cols = slice(part * span, (part + 1) * span)
         out_ref[:, cols] = (after_ref[:, cols].astype(F32) + (sums[:rows] + sums[rows:])).astype(BF16)
 
@@ -247,24 +283,38 @@
 
     gated = gate(conv_value, conv_gate)
     table = jnp.concatenate([conv_taps, conv_gain[None, :]], axis=0)
-    mixed = call(
-        conv_kernel, [VMEM] * 4, shape((owners, rows + PACK, width), F32),
-        [pltpu.VMEM((width // LANES, block_rows + 2 * HALO, LANES), F32)], 10**9, 16,
+    sent = call(
+        conv_kernel, [VMEM] * 4, shape((owners, rows + EXTRA, width), BF16),
+        [
+            pltpu.VMEM((width // LANES, block_rows + 2 * HALO, LANES), F32),
+            pltpu.VMEM((block_rows, width), F32),
+        ],
+        10**9, 8,
     )(gated, low, high, table)
-    near, _ = lax.optimization_barrier((near, mixed))
+    near, _ = lax.optimization_barrier((near, sent))
     half = lax.dynamic_slice_in_dim(near, core * half_width, half_width, 0)
     half = lax.ppermute(half, ("sp", "tp"), aside)
     swapped = lax.ppermute(near, "sp", swap)
     rest = lax.ppermute(half, "sp", swap)
-    mixed = lax.all_to_all(mixed, "tp", split_axis=0, concat_axis=0, tiled=True)
-
-    ids = expert_ids.T
+    mixed = lax.all_to_all(sent, "tp", split_axis=0, concat_axis=0, tiled=True)
+
+    ids, weights, _ = lax.optimization_barrier((expert_ids.T, expert_weights.T, sent))
+    pick, factor = call(
+        routing_kernel, [VMEM] * 2,
+        [shape((experts * PACK, parts * rows), BF16), shape((2 * parts * rows, experts * PACK), BF16)],
+        [], 10**9, 8,
+    )(ids, weights)
+    partial, act = call(
+        partial_kernel, [SMEM] + [VMEM] * 5,
+        [shape((rows, features), F32), shape((rows, half_width), BF16)],
+        [pltpu.VMEM((owners, rows, width), F32), pltpu.VMEM((owners, rows, width), BF16)],
+        10**9, 8,
+    )(jnp.stack([place, core]), mixed, point_weight, near, swapped, half)
     after, box = call(
-        dispatch_kernel, [SMEM] + [VMEM] * 9,
+        dispatch_kernel, [VMEM] * 6,
         [shape((rows, features), BF16), shape((experts * PACK, span), BF16)],
-        [pltpu.VMEM((owners, rows, width), BF16), pltpu.VMEM((parts * rows, span), BF16)],
-        10**9, 32,
-    )(jnp.stack([place, core]), mixed, latents, point_weight, near, swapped, half, rest, channel_gain[None, :], ids)
+        [pltpu.VMEM((parts * rows, span), BF16)], 10**9, 8,
+    )(latents, partial, act, rest, channel_gain[None, :], pick)
 
     box = box.reshape(members, PACK, span)
     arrived = lax.all_to_all(box, ("sp", "tp"), split_axis=0, concat_axis=0, tiled=True)
@@ -276,12 +326,12 @@
             pltpu.VMEM((members * cap, hidden_width), BF16),
             pltpu.VMEM((parts, members * cap, span), BF16),
         ],
-        5 * 10**9, 24,
+        5 * 10**9, 12,
     )(arrived.reshape(members * PACK, span), gate_weight[0], up_weight[0], down_weight[0])
     answer = answer.reshape(members, PACK, span)
     returned = lax.all_to_all(answer, ("sp", "tp"), split_axis=0, concat_axis=0, tiled=True)
-    return call(combine_kernel, [VMEM] * 4, shape((rows, features), BF16), [], 10**9, 32)(
-        returned.reshape(experts * PACK, span), after, ids, expert_weights.T
+    return call(combine_kernel, [VMEM] * 3, shape((rows, features), BF16), [], 10**9, 8)(
+        returned.reshape(experts * PACK, span), after, factor
     )
 
 

time: 289 us -> 286 us (0.990)
  starting transfers between devices: 44.8 us -> 37.4 us
    ppermute x1, waiting for transfers between devices: 1.32 us -> 8.4 us  [shards(): half = lax.ppermute(half, ('sp', 'tp'), aside)]
    ppermute x1, starting transfers between devices: 9.02 us -> 2.07 us  [shards(): rest = lax.ppermute(half, 'sp', swap)]
    all_to_all x1, waiting for transfers between devices: 9.74 us -> 4.23 us  [shards(): mixed = lax.all_to_all(sent, 'tp', split_axis=0, concat_axis=0, tiled=True)]
    ppermute x1, starting transfers between devices: 3.07 us -> 0.13 us  [shards(): half = lax.ppermute(half, ('sp', 'tp'), aside)]
    pallas_call x3 -> x5, Pallas kernels: 8.4 us -> 9.08 us  [the longest x1 2.35 us: shards(): call(dispatch_kernel, [VMEM] * 6, [shape((rows, features), BF16), shape((...]
  transfers between devices with their start and end apart: 7 -> 7, of which waited for: 2 -> 2; matrix products, arithmetic and copies ran while one was open for 1% -> 1% of each run, Pallas kernels for 1% -> 2%
where the time goes in v2:
time: 286 us
  blocking collectives  215 us (75%)
  starting transfers between devices  37.4 us (13%)
  Pallas kernels  15.2 us (5%)
  waiting for transfers between devices  12.6 us (4%)
    all_to_all x1, blocking collectives, shards(): lax.all_to_all(answer, ('sp', 'tp'), split_axis=0, concat_axis=0, tiled=T...  108 us
    all_to_all x1, blocking collectives, shards(): lax.all_to_all(box, ('sp', 'tp'), split_axis=0, concat_axis=0, tiled=True)  107 us
    ppermute x1, starting transfers between devices, shards(): high = lax.ppermute(gate(conv_value[:HALO], conv_gate[:HALO]), 'sp', behind)  18.7 us
    ppermute x1, waiting for transfers between devices, shards(): half = lax.ppermute(half, ('sp', 'tp'), aside)  8.4 us
    ppermute x1, starting transfers between devices, shards(): swapped = lax.ppermute(near, 'sp', swap)  7.36 us
    pallas_call x1, Pallas kernels, shards(): call(expert_kernel, [VMEM] * 4, shape((members * PACK, span), BF16), [plt...  6.15 us
  transfers between devices with their start and end apart: 7, of which 2 were waited for; matrix products, arithmetic and copies ran while one was open for 1% of the time, Pallas kernels for 2%

profile of v2, /device:TPU:33, one launch (start us, length us, event | category | flops | bytes accessed | tf_op | source)
XLA Modules:
  0.0 285.8 jit_solution(3442014632047231453)
XLA Ops:
  0.0 3.7 %collective-permute-start.2 = (bf16[256,2048]{1,0:T(8,128)(2,1)}, bf16[256,2048]{1,0:T(8,128)(2,1)S(1)}, u32[]{:S(2)}, u32[]{:S(2)}) collective-permute-start(bf16[256,2048]{1,0:T(8,128)(2,1)} %own_ref.1), channel_id=1, source_target_pairs={{0,1},{1,2},{2,3},{3,0},{4,7},{5,4},{6,5},{7,6},{8,9},{9,10},{10,1... | collective-permute-start | bytes 3145736 | tf_op jit(solution)/shard_map/ppermute | solution.py:282
  3.7 0.8 multiply_convert_fusion.1
  4.5 18.7 %collective-permute-start.1 = (bf16[16,256]{1,0:T(8,128)(2,1)S(1)}, bf16[16,256]{1,0:T(8,128)(2,1)S(1)}, u32[]{:S(2)}, u32[]{:S(2)}) collective-permute-start(bf16[16,256]{1,0:T(8,128)(2,1)S(1)} %get-tuple-element.23), channel_id=1, source_target_pairs={{4,0},{8,4},{12,8},{16,12},{20,16},{24,20},{28,24},{32,28},{36,32}... | collective-permute-start | bytes 24584 | tf_op jit(solution)/shard_map/ppermute | solution.py:271
  23.1 2.0 collective-permute-start
  25.1 1.2 multiply_convert_fusion.rows_ref
  26.3 0.8 pad_maximum_fusion.table_ref
  27.1 0.0 copy-start.9
  27.1 0.0 copy-start.10
  27.1 0.0 collective-permute-done.1.high_ref
  27.1 0.0 collective-permute-done.low_ref
  27.1 1.4 shard_map.118
  28.5 0.0 copy-start.3
  28.6 0.7 copy-done.3
  29.3 0.0 collective-permute-done.2.near_ref
  29.3 7.4 %collective-permute-start.3 = (bf16[256,2048]{1,0:T(8,128)(2,1)S(1)}, bf16[256,2048]{1,0:T(8,128)(2,1)S(1)}, u32[]{:S(2)}, u32[]{:S(2)}) collective-permute-start(bf16[256,2048]{1,0:T(8,128)(2,1)S(1)} %collective-permute-done.2.near_ref), channel_id=1, source_target_pairs={{0,4},{4,0},{8,12},{12,8},{16,20},{20,16},{24,28},{28,24},{32,36},... | collective-permute-start | bytes 3145736 | tf_op jit(solution)/shard_map/ppermute | solution.py:297
  36.7 0.0 copy-start
  36.7 0.1 collective-permute-start.4
  36.8 8.4 %collective-permute-done.4.half_ref = bf16[128,2048]{1,0:T(8,128)(2,1)} collective-permute-done((bf16[128,2048]{1,0:T(8,128)(2,1)S(1)}, bf16[128,2048]{1,0:T(8,128)(2,1)}, u32[]{:S(2)}, u32[]{:S(2)}) %collective-permute-start.4) | collective-permute-done | bytes 524320 | tf_op jit(solution)/shard_map/ppermute | solution.py:296
  45.2 2.1 collective-permute-start.5
  47.3 3.5 %all-to-all-start = ((bf16[4,144,256]{2,1,0:T(8,128)(2,1)}), bf16[4,144,256]{2,1,0:T(8,128)(2,1)S(1)}, u32[]{:S(2)}, u32[]{:S(2)}) async-start(bf16[4,144,256]{2,1,0:T(8,128)(2,1)} %copy-done.3), calls=%async_computation | async-start | bytes 589824 | tf_op jit(solution)/shard_map/all_to_all | solution.py:299
  50.9 0.1 pad_add_fusion.place_ref
  50.9 0.0 copy-done.9
  50.9 0.0 copy-done.10
  50.9 0.9 shard_map.120
  51.9 0.0 copy-start.1
  51.9 1.0 copy-done.1
  52.8 0.8 copy-done.11
  53.6 4.2 %all-to-all-done.mixed_ref = bf16[4,144,256]{2,1,0:T(8,128)(2,1)S(1)} async-done(((bf16[4,144,256]{2,1,0:T(8,128)(2,1)}), bf16[4,144,256]{2,1,0:T(8,128)(2,1)S(1)}, u32[]{:S(2)}, u32[]{:S(2)}) %all-to-all-start) | async-done | bytes 294944 | tf_op jit(solution)/shard_map/all_to_all | solution.py:299
  57.9 0.0 collective-permute-done.3.swapped_ref
  57.9 0.0 copy-done
  57.9 0.0 copy-start.6
  57.9 2.3 shard_map.119
  60.2 0.0 collective-permute-done.5.rest_ref
  60.2 0.0 copy-done.8
  60.3 0.0 copy-done.7
  60.3 0.0 copy-done.12
  60.3 0.0 copy-start.5
  60.3 2.3 shard_map.121
  62.6 0.0 copy-start.4
  62.7 107.3 %all_to_all.15 = bf16[128,8,1024]{2,1,0:T(8,128)(2,1)S(1)} all-to-all(bf16[128,8,1024]{2,1,0:T(8,128)(2,1)S(1)} %bitcast.14), channel_id=1, replica_groups=mesh['grp'=2,'sp'=32,'tp'=4] {'sp','tp'}, dimensions={0} | all-to-all | bytes 4194304 | tf_op jit(solution)/shard_map/all_to_all | solution.py:320
  169.9 0.0 copy-done.6
  169.9 0.0 copy-done.5
  169.9 0.0 copy-done.4
  169.9 6.2 %shard_map.122 = bf16[1024,1024]{1,0:T(8,128)(2,1)S(1)} custom-call(bf16[1024,1024]{1,0:T(8,128)(2,1)S(1)} %bitcast.15, bf16[2048,768]{1,0:T(8,128)(2,1)S(1)} %bitcast.17, bf16[2048,768]{1,0:T(8,128)(2,1)S(1)} %bitcast.18, bf16[768,2048]{1,0:T(8,128)(2,1)S(1)} %bitcast.19), custom_call_target="tpu_custom_call" | custom-call | flops 5000000000 | bytes 1048576 | tf_op jit(solution)/shard_map/pallas_call | solution.py:322
  176.1 0.0 copy-start.2
  176.1 107.6 %all_to_all.16 = bf16[128,8,1024]{2,1,0:T(8,128)(2,1)S(1)} all-to-all(bf16[128,8,1024]{2,1,0:T(8,128)(2,1)S(1)} %bitcast.16), channel_id=1, replica_groups=mesh['grp'=2,'sp'=32,'tp'=4] {'sp','tp'}, dimensions={0} | all-to-all | bytes 4194304 | tf_op jit(solution)/shard_map/all_to_all | solution.py:332
  283.7 0.0 copy-done.2
  283.7 2.0 shard_map.123
  (5 shorter events, 0.0 us)
Async XLA Ops:
  0.0 29.3 %collective-permute-start.2 = (bf16[256,2048]{1,0:T(8,128)(2,1)}, bf16[256,2048]{1,0:T(8,128)(2,1)S(1)}, u32[]{:S(2)}, u32[]{:S(2)}) collective-permute-start(bf16[256,2048]{1,0:T(8,128)(2,1)} %own_ref.1), channel_id=1, source_target_pairs={{0,1},{1,2},{2,3},{3,0},{4,7},{5,4},{6,5},{7,6},{8,9},{9,10},{10,1... | collective-permute-start | bytes 3145736 | tf_op jit(solution)/shard_map/ppermute | solution.py:282
  4.5 22.6 %collective-permute-start.1 = (bf16[16,256]{1,0:T(8,128)(2,1)S(1)}, bf16[16,256]{1,0:T(8,128)(2,1)S(1)}, u32[]{:S(2)}, u32[]{:S(2)}) collective-permute-start(bf16[16,256]{1,0:T(8,128)(2,1)S(1)} %get-tuple-element.23), channel_id=1, source_target_pairs={{4,0},{8,4},{12,8},{16,12},{20,16},{24,20},{28,24},{32,28},{36,32}... | collective-permute-start | bytes 24584 | tf_op jit(solution)/shard_map/ppermute | solution.py:271
  23.1 4.0 %collective-permute-start = (bf16[16,256]{1,0:T(8,128)(2,1)S(1)}, bf16[16,256]{1,0:T(8,128)(2,1)S(1)}, u32[]{:S(2)}, u32[]{:S(2)}) collective-permute-start(bf16[16,256]{1,0:T(8,128)(2,1)S(1)} %get-tuple-element.24), channel_id=1, source_target_pairs={{0,4},{4,8},{8,12},{12,16},{16,20},{20,24},{24,28},{28,32},{32,36}... | collective-permute-start | bytes 24584 | tf_op jit(solution)/shard_map/ppermute | solution.py:270
  27.1 23.9 %copy-start.9 = (s32[128,2]{0,1:T(2,128)S(1)}, s32[128,2]{0,1:T(2,128)}, u32[]{:S(2)}) copy-start(s32[128,2]{0,1:T(2,128)} %param.19) | copy-start | bytes 3076
  27.1 23.9 %copy-start.10 = (f32[128,2]{0,1:T(2,128)S(1)}, f32[128,2]{0,1:T(2,128)}, u32[]{:S(2)}) copy-start(f32[128,2]{0,1:T(2,128)} %param.20) | copy-start | bytes 3076
  28.5 0.7 copy-start.3
  29.3 28.6 %collective-permute-start.3 = (bf16[256,2048]{1,0:T(8,128)(2,1)S(1)}, bf16[256,2048]{1,0:T(8,128)(2,1)S(1)}, u32[]{:S(2)}, u32[]{:S(2)}) collective-permute-start(bf16[256,2048]{1,0:T(8,128)(2,1)S(1)} %collective-permute-done.2.near_ref), channel_id=1, source_target_pairs={{0,4},{4,0},{8,12},{12,8},{16,20},{20,16},{24,28},{28,24},{32,36},... | collective-permute-start | bytes 3145736 | tf_op jit(solution)/shard_map/ppermute | solution.py:297
  36.7 21.2 %copy-start = (bf16[256,2048]{1,0:T(8,128)(2,1)S(1)}, bf16[256,2048]{1,0:T(8,128)(2,1)}, u32[]{:S(2)}) copy-start(bf16[256,2048]{1,0:T(8,128)(2,1)} %own_ref.1) | copy-start | bytes 3145732
  36.7 8.5 %collective-permute-start.4 = (bf16[128,2048]{1,0:T(8,128)(2,1)S(1)}, bf16[128,2048]{1,0:T(8,128)(2,1)}, u32[]{:S(2)}, u32[]{:S(2)}) collective-permute-start(bf16[128,2048]{1,0:T(8,128)(2,1)S(1)} %constant_dynamic-slice_fusion), channel_id=1, source_target_pairs={{0,1},{1,2},{2,3},{3,0},{4,7},{5,4},{6,5},{7,6},{8,9},{9,10},{10,1... | collective-permute-start | bytes 1572872 | tf_op jit(solution)/shard_map/ppermute | solution.py:296
  45.2 15.0 %collective-permute-start.5 = (bf16[128,2048]{1,0:T(8,128)(2,1)}, bf16[128,2048]{1,0:T(8,128)(2,1)}, u32[]{:S(2)}, u32[]{:S(2)}) collective-permute-start(bf16[128,2048]{1,0:T(8,128)(2,1)} %collective-permute-done.4.half_ref), channel_id=1, source_target_pairs={{0,4},{4,0},{8,12},{12,8},{16,20},{20,16},{24,28},{28,24},{32,36},... | collective-permute-start | bytes 1572872 | tf_op jit(solution)/shard_map/ppermute | solution.py:298
  47.3 10.6 %all-to-all-start = ((bf16[4,144,256]{2,1,0:T(8,128)(2,1)}), bf16[4,144,256]{2,1,0:T(8,128)(2,1)S(1)}, u32[]{:S(2)}, u32[]{:S(2)}) async-start(bf16[4,144,256]{2,1,0:T(8,128)(2,1)} %copy-done.3), calls=%async_computation | async-start | bytes 589824 | tf_op jit(solution)/shard_map/all_to_all | solution.py:299
  51.9 1.0 copy-start.1
  52.8 0.8 copy-start.11
  53.6 6.6 %copy-start.8 = (f32[2048]{0:T(1024)S(1)}, f32[2048]{0:T(1024)}, u32[]{:S(2)}) copy-start(f32[2048]{0:T(1024)} %param.18) | copy-start | bytes 24580
  57.9 2.4 copy-start.7
  57.9 2.4 copy-start.12
  57.9 112.0 %copy-start.6 = (bf16[1,768,2048]{2,1,0:T(8,128)(2,1)S(1)}, bf16[1,768,2048]{2,1,0:T(8,128)(2,1)}, u32[]{:S(2)}) copy-start(bf16[1,768,2048]{2,1,0:T(8,128)(2,1)} %param.23) | copy-start | bytes 9437188
  60.3 109.6 %copy-start.5 = (bf16[1,2048,768]{2,1,0:T(8,128)(2,1)S(1)}, bf16[1,2048,768]{2,1,0:T(8,128)(2,1)}, u32[]{:S(2)}) copy-start(bf16[1,2048,768]{2,1,0:T(8,128)(2,1)} %param.22) | copy-start | bytes 9437188
  62.6 107.3 %copy-start.4 = (bf16[1,2048,768]{2,1,0:T(8,128)(2,1)S(1)}, bf16[1,2048,768]{2,1,0:T(8,128)(2,1)}, u32[]{:S(2)}) copy-start(bf16[1,2048,768]{2,1,0:T(8,128)(2,1)} %param.21) | copy-start | bytes 9437188
  176.1 107.6 %copy-start.2 = (bf16[512,1024]{1,0:T(8,128)(2,1)S(1)}, bf16[512,1024]{1,0:T(8,128)(2,1)}, u32[]{:S(2)}) copy-start(bf16[512,1024]{1,0:T(8,128)(2,1)} %copy-done.1) | copy-start | bytes 3145732

commit v3 on v2

--- a/solution.py
+++ b/solution.py
@@ -114,7 +114,23 @@
             factor_ref[first : first + rows] = jnp.where(here, value, 0.0).astype(BF16)
 
 
-def partial_kernel(place_ref, mixed_ref, own_ref, near_ref, swapped_ref, half_ref, out_ref, rest_ref, value_ref, act_ref):
+def halves_kernel(place_ref, weights_hbm, first_ref, second_ref, sems):
+    rows = first_ref.shape[0]
+    core = place_ref[1]
+    copies = []
+    for k, (half, out_ref) in enumerate(((core, first_ref), (1 - core, second_ref))):
+        source = weights_hbm.at[pl.ds(pl.multiple_of(half * rows, rows), rows)]
+        copies.append(pltpu.make_async_copy(source, out_ref, sems.at[k]))
+    for copy in copies:
+        copy.start()
+    for copy in copies:
+        copy.wait()
+
+
+def partial_kernel(
+    place_ref, mixed_ref, own_ref, near_a_ref, near_b_ref, far_a_ref, far_b_ref, half_ref,
+    out_ref, rest_ref, value_ref, act_ref,
+):
     owners, _, width = mixed_ref.shape
     rows, features = out_ref.shape
     half_width = width // 2
@@ -132,21 +148,26 @@
     scale = lax.rsqrt(squares / (owners * width) + 0.05)
     for j in range(owners):
         value = (value_ref[j] - center) * scale * joined(mixed_ref, j, rows)
-        act_ref[j] = (value * jax.nn.sigmoid(value)).astype(BF16)
+        value = (value * jax.nn.sigmoid(value)).astype(BF16)
+        act_ref[2 * j] = value[:, :half_width]
+        act_ref[2 * j + 1] = value[:, half_width:]
     place, core = place_ref[0], place_ref[1]
-    before = lax.rem(place + owners - 1 + 2 * core, owners)
-    beyond = lax.rem(place + owners + 1 - 2 * core, owners)
-    across = act_ref[lax.rem(place + 2, owners)]
-    lower, upper = across[:, :half_width], across[:, half_width:]
-    first = jnp.where(core == 0, lower, upper)
-    rest_ref[...] = jnp.where(core == 0, upper, lower)
+    before = 2 * lax.rem(place + owners - 1 + 2 * core, owners)
+    beyond = 2 * lax.rem(place + owners + 1 - 2 * core, owners)
+    across = 2 * lax.rem(place + 2, owners)
+    rest_ref[...] = act_ref[across + 1 - core]
+    pieces = (
+        (before + core, near_a_ref), (before + 1 - core, near_b_ref),
+        (beyond + 1 - core, far_a_ref), (beyond + core, far_b_ref), (across + core, half_ref),
+    )
     step = 512
     for start in range(0, features, step):
         cols = slice(start, start + step)
-        branch = dot(act_ref[place], own_ref[:, cols])
-        branch = branch + dot(act_ref[before], near_ref[:, cols])
-        branch = branch + dot(act_ref[beyond], swapped_ref[:, cols])
-        out_ref[:, cols] = branch + dot(first, half_ref[:, cols])
+        branch = dot(act_ref[2 * place], own_ref[:half_width, cols])
+        branch = branch + dot(act_ref[2 * place + 1], own_ref[half_width:, cols])
+        for index, piece_ref in pieces:
+            branch = branch + dot(act_ref[index], piece_ref[:, cols])
+        out_ref[:, cols] = branch
 
 
 def dispatch_kernel(
@@ -235,6 +256,7 @@
 
 VMEM = pl.BlockSpec(memory_space=pltpu.VMEM)
 SMEM = pl.BlockSpec(memory_space=pltpu.SMEM)
+ANY = pl.BlockSpec(memory_space=pl.ANY)
 
 
 def call(kernel, specs, outs, scratch, flops, size):
@@ -279,7 +301,13 @@
         for i in range(owners)
     ]
     swap = [(i, i ^ 1) for i in range(stages)]
-    near = lax.ppermute(point_weight, ("sp", "tp"), aside)
+    whereabouts = jnp.stack([place, core])
+    piece = shape((half_width, features), BF16)
+    leading, trailing = call(
+        halves_kernel, [SMEM, ANY], [piece, piece], [pltpu.SemaphoreType.DMA((2,))], 10**6, 4
+    )(whereabouts, point_weight)
+    near_a = lax.ppermute(leading, ("sp", "tp"), aside)
+    near_b = lax.ppermute(trailing, ("sp", "tp"), aside)
 
     gated = gate(conv_value, conv_gate)
     table = jnp.concatenate([conv_taps, conv_gain[None, :]], axis=0)
@@ -291,10 +319,10 @@
         ],
         10**9, 8,
     )(gated, low, high, table)
-    near, _ = lax.optimization_barrier((near, sent))
-    half = lax.dynamic_slice_in_dim(near, core * half_width, half_width, 0)
-    half = lax.ppermute(half, ("sp", "tp"), aside)
-    swapped = lax.ppermute(near, "sp", swap)
+    near_a, _ = lax.optimization_barrier((near_a, sent))
+    half = lax.ppermute(near_a, ("sp", "tp"), aside)
+    far_a = lax.ppermute(near_a, "sp", swap)
+    far_b = lax.ppermute(near_b, "sp", swap)
     rest = lax.ppermute(half, "sp", swap)
     mixed = lax.all_to_all(sent, "tp", split_axis=0, concat_axis=0, tiled=True)
 
@@ -305,11 +333,11 @@
         [], 10**9, 8,
     )(ids, weights)
     partial, act = call(
-        partial_kernel, [SMEM] + [VMEM] * 5,
+        partial_kernel, [SMEM] + [VMEM] * 7,
         [shape((rows, features), F32), shape((rows, half_width), BF16)],
-        [pltpu.VMEM((owners, rows, width), F32), pltpu.VMEM((owners, rows, width), BF16)],
+        [pltpu.VMEM((owners, rows, width), F32), pltpu.VMEM((2 * owners, rows, half_width), BF16)],
         10**9, 8,
-    )(jnp.stack([place, core]), mixed, point_weight, near, swapped, half)
+    )(whereabouts, mixed, point_weight, near_a, near_b, far_a, far_b, half)
     after, box = call(
         dispatch_kernel, [VMEM] * 6,
         [shape((rows, features), BF16), shape((experts * PACK, span), BF16)],

time: 286 us -> 286 us (level)
    ppermute x3 -> x5, waiting for transfers between devices: 8.41 us -> 6.15 us  [the longest x1 4.47 us: shards(): half = lax.ppermute(near_a, ('sp', 'tp'), aside)]
    ppermute x3 -> x5, starting transfers between devices: 11.2 us -> 9.14 us  [the longest x1 3.82 us: shards(): near_a = lax.ppermute(leading, ('sp', 'tp'), aside)]
  transfers between devices with their start and end apart: 7 -> 9, of which waited for: 2 -> 3; matrix products, arithmetic and copies ran while one was open for 1% -> 1% of each run, Pallas kernels for 2% -> 2%
where the time goes in v3:
time: 286 us
  blocking collectives  217 us (76%)
  starting transfers between devices  34.6 us (12%)
  Pallas kernels  17.5 us (6%)
  waiting for transfers between devices  11.4 us (4%)
    all_to_all x1, blocking collectives, shards(): lax.all_to_all(box, ('sp', 'tp'), split_axis=0, concat_axis=0, tiled=True)  110 us
    all_to_all x1, blocking collectives, shards(): lax.all_to_all(answer, ('sp', 'tp'), split_axis=0, concat_axis=0, tiled=T...  107 us
    ppermute x1, starting transfers between devices, shards(): high = lax.ppermute(gate(conv_value[:HALO], conv_gate[:HALO]), 'sp', behind)  18.7 us
    pallas_call x1, Pallas kernels, shards(): call(expert_kernel, [VMEM] * 4, shape((members * PACK, span), BF16), [plt...  6.15 us
  transfers between devices with their start and end apart: 9, of which 3 were waited for; matrix products, arithmetic and copies ran while one was open for 1% of the time, Pallas kernels for 2%

profile of v3, /device:TPU:33, one launch (start us, length us, event | category | flops | bytes accessed | tf_op | source)
XLA Modules:
  0.0 285.9 jit_solution(8924169111733272692)
XLA Ops:
  0.0 0.1 pad_add_fusion.place_ref
  0.1 0.0 copy-start
  0.1 1.2 copy-done
  1.3 0.6 shard_map.119
  1.9 3.8 %collective-permute-start.2 = (bf16[128,2048]{1,0:T(8,128)(2,1)S(1)}, bf16[128,2048]{1,0:T(8,128)(2,1)S(1)}, u32[]{:S(2)}, u32[]{:S(2)}) collective-permute-start(bf16[128,2048]{1,0:T(8,128)(2,1)S(1)} %get-tuple-element.16), channel_id=1, source_target_pairs={{0,1},{1,2},{2,3},{3,0},{4,7},{5,4},{6,5},{7,6},{8,9},{9,10},{10,1... | collective-permute-start | bytes 1572872 | tf_op jit(solution)/shard_map/ppermute | solution.py:309
  5.8 0.8 multiply_convert_fusion.1
  6.5 18.7 %collective-permute-start.1 = (bf16[16,256]{1,0:T(8,128)(2,1)S(1)}, bf16[16,256]{1,0:T(8,128)(2,1)S(1)}, u32[]{:S(2)}, u32[]{:S(2)}) collective-permute-start(bf16[16,256]{1,0:T(8,128)(2,1)S(1)} %get-tuple-element.27), channel_id=1, source_target_pairs={{4,0},{8,4},{12,8},{16,12},{20,16},{24,20},{28,24},{32,28},{36,32}... | collective-permute-start | bytes 24584 | tf_op jit(solution)/shard_map/ppermute | solution.py:293
  25.2 2.0 collective-permute-start
  27.2 3.0 %collective-permute-start.3 = (bf16[128,2048]{1,0:T(8,128)(2,1)S(1)}, bf16[128,2048]{1,0:T(8,128)(2,1)S(1)}, u32[]{:S(2)}, u32[]{:S(2)}) collective-permute-start(bf16[128,2048]{1,0:T(8,128)(2,1)S(1)} %get-tuple-element.18), channel_id=1, source_target_pairs={{0,1},{1,2},{2,3},{3,0},{4,7},{5,4},{6,5},{7,6},{8,9},{9,10},{10,1... | collective-permute-start | bytes 1572872 | tf_op jit(solution)/shard_map/ppermute | solution.py:310
  30.2 1.2 multiply_convert_fusion.rows_ref
  31.4 0.8 pad_maximum_fusion.table_ref
  32.2 0.0 copy-start.7
  32.2 0.0 collective-permute-done.1.high_ref
  32.2 0.0 collective-permute-done.low_ref
  32.2 2.3 shard_map.118
  34.5 0.0 collective-permute-done.2.near_a_ref
  34.5 0.0 collective-permute-start.6
  34.5 0.1 collective-permute-start.4
  34.7 1.7 collective-permute-done.3.near_b_ref
  36.3 2.1 collective-permute-start.5
  38.5 4.5 %collective-permute-done.6.half_ref = bf16[128,2048]{1,0:T(8,128)(2,1)} collective-permute-done((bf16[128,2048]{1,0:T(8,128)(2,1)S(1)}, bf16[128,2048]{1,0:T(8,128)(2,1)}, u32[]{:S(2)}, u32[]{:S(2)}) %collective-permute-start.6) | collective-permute-done | bytes 524320 | tf_op jit(solution)/shard_map/ppermute | solution.py:323
  43.0 1.3 collective-permute-start.7
  44.2 3.5 %all-to-all-start = ((bf16[4,144,256]{2,1,0:T(8,128)(2,1)}), bf16[4,144,256]{2,1,0:T(8,128)(2,1)S(1)}, u32[]{:S(2)}, u32[]{:S(2)}) async-start(bf16[4,144,256]{2,1,0:T(8,128)(2,1)} %shard_map.118), calls=%async_computation | async-start | bytes 589824 | tf_op jit(solution)/shard_map/all_to_all | solution.py:327
  47.8 0.0 copy-done.7
  47.8 0.0 copy-done.8
  47.8 0.9 shard_map.121
  48.7 0.0 copy-start.9
  48.7 0.8 copy-done.9
  49.5 5.3 %all-to-all-done.mixed_ref = bf16[4,144,256]{2,1,0:T(8,128)(2,1)S(1)} async-done(((bf16[4,144,256]{2,1,0:T(8,128)(2,1)}), bf16[4,144,256]{2,1,0:T(8,128)(2,1)S(1)}, u32[]{:S(2)}, u32[]{:S(2)}) %all-to-all-start) | async-done | bytes 294944 | tf_op jit(solution)/shard_map/all_to_all | solution.py:327
  54.8 0.0 collective-permute-done.4.far_a_ref
  54.8 0.0 collective-permute-done.5.far_b_ref
  54.8 0.0 copy-done.1
  54.8 0.0 copy-start.4
  54.8 3.1 %shard_map.120 = (f32[128,2048]{1,0:T(8,128)S(1)}, bf16[128,128]{1,0:T(8,128)(2,1)S(1)}) custom-call(s32[2]{0:T(128)S(1)} %pad_add_fusion.place_ref, bf16[4,144,256]{2,1,0:T(8,128)(2,1)S(1)} %all-to-all-done.mixed_ref, bf16[256,2048]{1,0:T(8,128)(2,1)S(1)} %copy-done.1, bf16[128,2048]{1,0:T(8,128)(2,1)S(1)} %collective-permute-done.2.near_a_ref, ...), custom_call_target="tpu_custom_call" | custom-call | flops 1000000000 | bytes 1048576 | tf_op jit(solution)/shard_map/pallas_call | solution.py:335
  58.0 0.0 collective-permute-done.7.rest_ref
  58.0 0.0 copy-done.6
  58.0 0.0 copy-done.5
  58.0 0.0 copy-done.10
  58.0 0.0 copy-start.3
  58.0 2.3 shard_map.122
  60.4 0.0 copy-start.2
  60.4 109.8 %all_to_all.15 = bf16[128,8,1024]{2,1,0:T(8,128)(2,1)S(1)} all-to-all(bf16[128,8,1024]{2,1,0:T(8,128)(2,1)S(1)} %bitcast.14), channel_id=1, replica_groups=mesh['grp'=2,'sp'=32,'tp'=4] {'sp','tp'}, dimensions={0} | all-to-all | bytes 4194304 | tf_op jit(solution)/shard_map/all_to_all | solution.py:348
  170.1 0.0 copy-done.4
  170.1 0.0 copy-done.3
  170.1 0.0 copy-done.2
  170.1 6.2 %shard_map.123 = bf16[1024,1024]{1,0:T(8,128)(2,1)S(1)} custom-call(bf16[1024,1024]{1,0:T(8,128)(2,1)S(1)} %bitcast.15, bf16[2048,768]{1,0:T(8,128)(2,1)S(1)} %bitcast.17, bf16[2048,768]{1,0:T(8,128)(2,1)S(1)} %bitcast.18, bf16[768,2048]{1,0:T(8,128)(2,1)S(1)} %bitcast.19), custom_call_target="tpu_custom_call" | custom-call | flops 5000000000 | bytes 1048576 | tf_op jit(solution)/shard_map/pallas_call | solution.py:350
  176.3 107.5 %all_to_all.16 = bf16[128,8,1024]{2,1,0:T(8,128)(2,1)S(1)} all-to-all(bf16[128,8,1024]{2,1,0:T(8,128)(2,1)S(1)} %bitcast.16), channel_id=1, replica_groups=mesh['grp'=2,'sp'=32,'tp'=4] {'sp','tp'}, dimensions={0} | all-to-all | bytes 4194304 | tf_op jit(solution)/shard_map/all_to_all | solution.py:360
  283.8 2.0 shard_map.124
  (5 shorter events, 0.0 us)
Async XLA Ops:
  0.1 1.2 copy-start
  1.9 32.6 %collective-permute-start.2 = (bf16[128,2048]{1,0:T(8,128)(2,1)S(1)}, bf16[128,2048]{1,0:T(8,128)(2,1)S(1)}, u32[]{:S(2)}, u32[]{:S(2)}) collective-permute-start(bf16[128,2048]{1,0:T(8,128)(2,1)S(1)} %get-tuple-element.16), channel_id=1, source_target_pairs={{0,1},{1,2},{2,3},{3,0},{4,7},{5,4},{6,5},{7,6},{8,9},{9,10},{10,1... | collective-permute-start | bytes 1572872 | tf_op jit(solution)/shard_map/ppermute | solution.py:309
  6.5 25.7 %collective-permute-start.1 = (bf16[16,256]{1,0:T(8,128)(2,1)S(1)}, bf16[16,256]{1,0:T(8,128)(2,1)S(1)}, u32[]{:S(2)}, u32[]{:S(2)}) collective-permute-start(bf16[16,256]{1,0:T(8,128)(2,1)S(1)} %get-tuple-element.27), channel_id=1, source_target_pairs={{4,0},{8,4},{12,8},{16,12},{20,16},{24,20},{28,24},{32,28},{36,32}... | collective-permute-start | bytes 24584 | tf_op jit(solution)/shard_map/ppermute | solution.py:293
  25.2 7.0 %collective-permute-start = (bf16[16,256]{1,0:T(8,128)(2,1)S(1)}, bf16[16,256]{1,0:T(8,128)(2,1)S(1)}, u32[]{:S(2)}, u32[]{:S(2)}) collective-permute-start(bf16[16,256]{1,0:T(8,128)(2,1)S(1)} %get-tuple-element.28), channel_id=1, source_target_pairs={{0,4},{4,8},{8,12},{12,16},{16,20},{20,24},{24,28},{28,32},{32,36}... | collective-permute-start | bytes 24584 | tf_op jit(solution)/shard_map/ppermute | solution.py:292
  27.2 9.2 %collective-permute-start.3 = (bf16[128,2048]{1,0:T(8,128)(2,1)S(1)}, bf16[128,2048]{1,0:T(8,128)(2,1)S(1)}, u32[]{:S(2)}, u32[]{:S(2)}) collective-permute-start(bf16[128,2048]{1,0:T(8,128)(2,1)S(1)} %get-tuple-element.18), channel_id=1, source_target_pairs={{0,1},{1,2},{2,3},{3,0},{4,7},{5,4},{6,5},{7,6},{8,9},{9,10},{10,1... | collective-permute-start | bytes 1572872 | tf_op jit(solution)/shard_map/ppermute | solution.py:310
  32.2 15.6 %copy-start.7 = (s32[128,2]{0,1:T(2,128)S(1)}, s32[128,2]{0,1:T(2,128)}, u32[]{:S(2)}) copy-start(s32[128,2]{0,1:T(2,128)} %param.19) | copy-start | bytes 3076
  32.2 15.6 %copy-start.8 = (f32[128,2]{0,1:T(2,128)S(1)}, f32[128,2]{0,1:T(2,128)}, u32[]{:S(2)}) copy-start(f32[128,2]{0,1:T(2,128)} %param.20) | copy-start | bytes 3076
  34.5 20.3 %copy-start.1 = (bf16[256,2048]{1,0:T(8,128)(2,1)S(1)}, bf16[256,2048]{1,0:T(8,128)(2,1)}, u32[]{:S(2)}) copy-start(bf16[256,2048]{1,0:T(8,128)(2,1)} %own_ref.1) | copy-start | bytes 3145732
  34.5 8.4 %collective-permute-start.6 = (bf16[128,2048]{1,0:T(8,128)(2,1)S(1)}, bf16[128,2048]{1,0:T(8,128)(2,1)}, u32[]{:S(2)}, u32[]{:S(2)}) collective-permute-start(bf16[128,2048]{1,0:T(8,128)(2,1)S(1)} %collective-permute-done.2.near_a_ref), channel_id=1, source_target_pairs={{0,1},{1,2},{2,3},{3,0},{4,7},{5,4},{6,5},{7,6},{8,9},{9,10},{10,1... | collective-permute-start | bytes 1572872 | tf_op jit(solution)/shard_map/ppermute | solution.py:323
  34.5 20.2 %collective-permute-start.4 = (bf16[128,2048]{1,0:T(8,128)(2,1)S(1)}, bf16[128,2048]{1,0:T(8,128)(2,1)}, u32[]{:S(2)}, u32[]{:S(2)}) collective-permute-start(bf16[128,2048]{1,0:T(8,128)(2,1)S(1)} %collective-permute-done.2.near_a_ref), channel_id=1, source_target_pairs={{0,4},{4,0},{8,12},{12,8},{16,20},{20,16},{24,28},{28,24},{32,36},... | collective-permute-start | bytes 1572872 | tf_op jit(solution)/shard_map/ppermute | solution.py:324
  36.3 18.4 %collective-permute-start.5 = (bf16[128,2048]{1,0:T(8,128)(2,1)S(1)}, bf16[128,2048]{1,0:T(8,128)(2,1)}, u32[]{:S(2)}, u32[]{:S(2)}) collective-permute-start(bf16[128,2048]{1,0:T(8,128)(2,1)S(1)} %collective-permute-done.3.near_b_ref), channel_id=1, source_target_pairs={{0,4},{4,0},{8,12},{12,8},{16,20},{20,16},{24,28},{28,24},{32,36},... | collective-permute-start | bytes 1572872 | tf_op jit(solution)/shard_map/ppermute | solution.py:325
  43.0 15.0 %collective-permute-start.7 = (bf16[128,2048]{1,0:T(8,128)(2,1)}, bf16[128,2048]{1,0:T(8,128)(2,1)}, u32[]{:S(2)}, u32[]{:S(2)}) collective-permute-start(bf16[128,2048]{1,0:T(8,128)(2,1)} %collective-permute-done.6.half_ref), channel_id=1, source_target_pairs={{0,4},{4,0},{8,12},{12,8},{16,20},{20,16},{24,28},{28,24},{32,36},... | collective-permute-start | bytes 1572872 | tf_op jit(solution)/shard_map/ppermute | solution.py:326
  44.2 10.6 %all-to-all-start = ((bf16[4,144,256]{2,1,0:T(8,128)(2,1)}), bf16[4,144,256]{2,1,0:T(8,128)(2,1)S(1)}, u32[]{:S(2)}, u32[]{:S(2)}) async-start(bf16[4,144,256]{2,1,0:T(8,128)(2,1)} %shard_map.118), calls=%async_computation | async-start | bytes 589824 | tf_op jit(solution)/shard_map/all_to_all | solution.py:327
  48.7 0.8 copy-start.9
  49.5 8.5 %copy-start.6 = (f32[2048]{0:T(1024)S(1)}, f32[2048]{0:T(1024)}, u32[]{:S(2)}) copy-start(f32[2048]{0:T(1024)} %param.18) | copy-start | bytes 24580
  54.8 3.2 %copy-start.5 = (bf16[128,2048]{1,0:T(8,128)(2,1)S(1)}, bf16[128,2048]{1,0:T(8,128)(2,1)}, u32[]{:S(2)}) copy-start(bf16[128,2048]{1,0:T(8,128)(2,1)} %latents_ref.1) | copy-start | bytes 1572868
  54.8 3.2 %copy-start.10 = (bf16[1024,256]{1,0:T(8,128)(2,1)S(1)}, bf16[1024,256]{1,0:T(8,128)(2,1)}, u32[]{:S(2)}) copy-start(bf16[1024,256]{1,0:T(8,128)(2,1)} %copy-done.9) | copy-start | bytes 1572868
  54.8 115.3 %copy-start.4 = (bf16[1,768,2048]{2,1,0:T(8,128)(2,1)S(1)}, bf16[1,768,2048]{2,1,0:T(8,128)(2,1)}, u32[]{:S(2)}) copy-start(bf16[1,768,2048]{2,1,0:T(8,128)(2,1)} %param.23) | copy-start | bytes 9437188
  58.0 112.1 %copy-start.3 = (bf16[1,2048,768]{2,1,0:T(8,128)(2,1)S(1)}, bf16[1,2048,768]{2,1,0:T(8,128)(2,1)}, u32[]{:S(2)}) copy-start(bf16[1,2048,768]{2,1,0:T(8,128)(2,1)} %param.22) | copy-start | bytes 9437188
  60.4 109.8 %copy-start.2 = (bf16[1,2048,768]{2,1,0:T(8,128)(2,1)S(1)}, bf16[1,2048,768]{2,1,0:T(8,128)(2,1)}, u32[]{:S(2)}) copy-start(bf16[1,2048,768]{2,1,0:T(8,128)(2,1)} %param.21) | copy-start | bytes 9437188

commit v4 on v2

--- a/solution.py
+++ b/solution.py
@@ -114,7 +114,9 @@
             factor_ref[first : first + rows] = jnp.where(here, value, 0.0).astype(BF16)
 
 
-def partial_kernel(place_ref, mixed_ref, own_ref, near_ref, swapped_ref, half_ref, out_ref, rest_ref, value_ref, act_ref):
+def partial_kernel(
+    place_ref, mixed_ref, own_ref, near_ref, swapped_ref, out_ref, first_ref, second_ref, value_ref, act_ref
+):
     owners, _, width = mixed_ref.shape
     rows, features = out_ref.shape
     half_width = width // 2
@@ -138,26 +140,27 @@
     beyond = lax.rem(place + owners + 1 - 2 * core, owners)
     across = act_ref[lax.rem(place + 2, owners)]
     lower, upper = across[:, :half_width], across[:, half_width:]
-    first = jnp.where(core == 0, lower, upper)
-    rest_ref[...] = jnp.where(core == 0, upper, lower)
+    first_ref[...] = jnp.where(core == 0, lower, upper)
+    second_ref[...] = jnp.where(core == 0, upper, lower)
     step = 512
     for start in range(0, features, step):
         cols = slice(start, start + step)
         branch = dot(act_ref[place], own_ref[:, cols])
         branch = branch + dot(act_ref[before], near_ref[:, cols])
-        branch = branch + dot(act_ref[beyond], swapped_ref[:, cols])
-        out_ref[:, cols] = branch + dot(first, half_ref[:, cols])
+        out_ref[:, cols] = branch + dot(act_ref[beyond], swapped_ref[:, cols])
 
 
 def dispatch_kernel(
-    latents_ref, partial_ref, act_ref, rest_ref, gain_ref, pick_ref, after_ref, box_ref, x_ref
+    latents_ref, partial_ref, first_ref, second_ref, half_ref, rest_ref, gain_ref, pick_ref,
+    after_ref, box_ref, x_ref,
 ):
     rows, features = latents_ref.shape
     step = 512
     squares = jnp.zeros((rows, 1), F32)
     for start in range(0, features, step):
         cols = slice(start, start + step)
-        branch = partial_ref[:, cols] + dot(act_ref[...], rest_ref[:, cols])
+        branch = partial_ref[:, cols] + dot(first_ref[...], half_ref[:, cols])
+        branch = branch + dot(second_ref[...], rest_ref[:, cols])
         after = (latents_ref[:, cols].astype(F32) + branch).astype(BF16)
         after_ref[:, cols] = after
         after = after.astype(F32)
@@ -304,17 +307,17 @@
         [shape((experts * PACK, parts * rows), BF16), shape((2 * parts * rows, experts * PACK), BF16)],
         [], 10**9, 8,
     )(ids, weights)
-    partial, act = call(
-        partial_kernel, [SMEM] + [VMEM] * 5,
-        [shape((rows, features), F32), shape((rows, half_width), BF16)],
+    partial, first, second = call(
+        partial_kernel, [SMEM] + [VMEM] * 4,
+        [shape((rows, features), F32)] + [shape((rows, half_width), BF16)] * 2,
         [pltpu.VMEM((owners, rows, width), F32), pltpu.VMEM((owners, rows, width), BF16)],
         10**9, 8,
-    )(jnp.stack([place, core]), mixed, point_weight, near, swapped, half)
+    )(jnp.stack([place, core]), mixed, point_weight, near, swapped)
     after, box = call(
-        dispatch_kernel, [VMEM] * 6,
+        dispatch_kernel, [VMEM] * 8,
         [shape((rows, features), BF16), shape((experts * PACK, span), BF16)],
         [pltpu.VMEM((parts * rows, span), BF16)], 10**9, 8,
-    )(latents, partial, act, rest, channel_gain[None, :], pick)
+    )(latents, partial, first, second, half, rest, channel_gain[None, :], pick)
 
     box = box.reshape(members, PACK, span)
     arrived = lax.all_to_all(box, ("sp", "tp"), split_axis=0, concat_axis=0, tiled=True)

time: 286 us -> 286 us (level)
  no operation moved by 1% of the time
where the time goes in v4:
time: 286 us
  blocking collectives  215 us (75%)
  starting transfers between devices  37.4 us (13%)
  Pallas kernels  16.3 us (6%)
  waiting for transfers between devices  13.6 us (5%)
    all_to_all x1, blocking collectives, shards(): lax.all_to_all(answer, ('sp', 'tp'), split_axis=0, concat_axis=0, tiled=T...  107 us
    all_to_all x1, blocking collectives, shards(): lax.all_to_all(box, ('sp', 'tp'), split_axis=0, concat_axis=0, tiled=True)  107 us
    ppermute x1, starting transfers between devices, shards(): high = lax.ppermute(gate(conv_value[:HALO], conv_gate[:HALO]), 'sp', behind)  18.7 us
    ppermute x1, waiting for transfers between devices, shards(): half = lax.ppermute(half, ('sp', 'tp'), aside)  8.4 us
    ppermute x1, starting transfers between devices, shards(): swapped = lax.ppermute(near, 'sp', swap)  7.36 us
    pallas_call x1, Pallas kernels, shards(): call(expert_kernel, [VMEM] * 4, shape((members * PACK, span), BF16), [plt...  6.15 us
  transfers between devices with their start and end apart: 7, of which 2 were waited for; matrix products, arithmetic and copies ran while one was open for 1% of the time, Pallas kernels for 2%

profile of v4, /device:TPU:33, one launch (start us, length us, event | category | flops | bytes accessed | tf_op | source)
XLA Modules:
  0.0 286.0 jit_solution(5621576613038486224)
XLA Ops:
  0.0 3.7 %collective-permute-start.2 = (bf16[256,2048]{1,0:T(8,128)(2,1)}, bf16[256,2048]{1,0:T(8,128)(2,1)S(1)}, u32[]{:S(2)}, u32[]{:S(2)}) collective-permute-start(bf16[256,2048]{1,0:T(8,128)(2,1)} %own_ref.1), channel_id=1, source_target_pairs={{0,1},{1,2},{2,3},{3,0},{4,7},{5,4},{6,5},{7,6},{8,9},{9,10},{10,1... | collective-permute-start | bytes 3145736 | tf_op jit(solution)/shard_map/ppermute | solution.py:285
  3.7 0.8 multiply_convert_fusion.1
  4.5 18.7 %collective-permute-start.1 = (bf16[16,256]{1,0:T(8,128)(2,1)S(1)}, bf16[16,256]{1,0:T(8,128)(2,1)S(1)}, u32[]{:S(2)}, u32[]{:S(2)}) collective-permute-start(bf16[16,256]{1,0:T(8,128)(2,1)S(1)} %get-tuple-element.25), channel_id=1, source_target_pairs={{4,0},{8,4},{12,8},{16,12},{20,16},{24,20},{28,24},{32,28},{36,32}... | collective-permute-start | bytes 24584 | tf_op jit(solution)/shard_map/ppermute | solution.py:274
  23.1 2.0 collective-permute-start
  25.1 1.2 multiply_convert_fusion.rows_ref
  26.3 0.8 pad_maximum_fusion.table_ref
  27.1 0.0 copy-start.6
  27.1 0.0 copy-start.7
  27.1 0.0 collective-permute-done.1.high_ref
  27.1 0.0 collective-permute-done.low_ref
  27.1 2.2 shard_map.118
  29.3 0.0 collective-permute-done.2.near_ref
  29.3 7.4 %collective-permute-start.3 = (bf16[256,2048]{1,0:T(8,128)(2,1)S(1)}, bf16[256,2048]{1,0:T(8,128)(2,1)}, u32[]{:S(2)}, u32[]{:S(2)}) collective-permute-start(bf16[256,2048]{1,0:T(8,128)(2,1)S(1)} %collective-permute-done.2.near_ref), channel_id=1, source_target_pairs={{0,4},{4,0},{8,12},{12,8},{16,20},{20,16},{24,28},{28,24},{32,36},... | collective-permute-start | bytes 3145736 | tf_op jit(solution)/shard_map/ppermute | solution.py:300
  36.7 0.0 copy-start.3
  36.7 0.1 collective-permute-start.4
  36.8 8.4 %collective-permute-done.4.half_ref = bf16[128,2048]{1,0:T(8,128)(2,1)} collective-permute-done((bf16[128,2048]{1,0:T(8,128)(2,1)S(1)}, bf16[128,2048]{1,0:T(8,128)(2,1)}, u32[]{:S(2)}, u32[]{:S(2)}) %collective-permute-start.4) | collective-permute-done | bytes 524320 | tf_op jit(solution)/shard_map/ppermute | solution.py:299
  45.2 2.1 collective-permute-start.5
  47.3 3.5 %all-to-all-start = ((bf16[4,144,256]{2,1,0:T(8,128)(2,1)}), bf16[4,144,256]{2,1,0:T(8,128)(2,1)S(1)}, u32[]{:S(2)}, u32[]{:S(2)}) async-start(bf16[4,144,256]{2,1,0:T(8,128)(2,1)} %shard_map.118), calls=%async_computation | async-start | bytes 589824 | tf_op jit(solution)/shard_map/all_to_all | solution.py:302
  50.9 0.1 pad_add_fusion.place_ref
  50.9 0.0 copy-done.6
  50.9 0.0 copy-done.7
  50.9 0.9 shard_map.120
  51.9 0.0 copy-start.8
  51.9 0.8 copy-done.8
  52.7 0.0 copy-start.5
  52.7 5.2 %all-to-all-done.mixed_ref = bf16[4,144,256]{2,1,0:T(8,128)(2,1)S(1)} async-done(((bf16[4,144,256]{2,1,0:T(8,128)(2,1)}), bf16[4,144,256]{2,1,0:T(8,128)(2,1)S(1)}, u32[]{:S(2)}, u32[]{:S(2)}) %all-to-all-start) | async-done | bytes 294944 | tf_op jit(solution)/shard_map/all_to_all | solution.py:302
  57.9 0.0 copy-start.4
  57.9 0.0 copy-start.9
  57.9 0.0 collective-permute-done.3.swapped_ref
  57.9 0.0 copy-done.3
  57.9 0.0 copy-start.2
  57.9 2.4 shard_map.119
  60.3 0.0 collective-permute-done.5.rest_ref
  60.3 0.0 copy-done.5
  60.3 0.0 copy-done.4
  60.3 0.0 copy-done.9
  60.4 0.0 copy-start.1
  60.4 2.6 shard_map.121
  63.0 0.0 copy-start
  63.0 107.3 %all_to_all.15 = bf16[128,8,1024]{2,1,0:T(8,128)(2,1)S(1)} all-to-all(bf16[128,8,1024]{2,1,0:T(8,128)(2,1)S(1)} %bitcast.14), channel_id=1, replica_groups=mesh['grp'=2,'sp'=32,'tp'=4] {'sp','tp'}, dimensions={0} | all-to-all | bytes 4194304 | tf_op jit(solution)/shard_map/all_to_all | solution.py:323
  170.3 0.0 copy-done.2
  170.3 0.0 copy-done.1
  170.3 0.0 copy-done
  170.3 6.2 %shard_map.122 = bf16[1024,1024]{1,0:T(8,128)(2,1)S(1)} custom-call(bf16[1024,1024]{1,0:T(8,128)(2,1)S(1)} %bitcast.15, bf16[2048,768]{1,0:T(8,128)(2,1)S(1)} %bitcast.17, bf16[2048,768]{1,0:T(8,128)(2,1)S(1)} %bitcast.18, bf16[768,2048]{1,0:T(8,128)(2,1)S(1)} %bitcast.19), custom_call_target="tpu_custom_call" | custom-call | flops 5000000000 | bytes 1048576 | tf_op jit(solution)/shard_map/pallas_call | solution.py:325
  176.5 107.5 %all_to_all.16 = bf16[128,8,1024]{2,1,0:T(8,128)(2,1)S(1)} all-to-all(bf16[128,8,1024]{2,1,0:T(8,128)(2,1)S(1)} %bitcast.16), channel_id=1, replica_groups=mesh['grp'=2,'sp'=32,'tp'=4] {'sp','tp'}, dimensions={0} | all-to-all | bytes 4194304 | tf_op jit(solution)/shard_map/all_to_all | solution.py:335
  283.9 2.0 shard_map.123
  (1 shorter events, 0.0 us)
Async XLA Ops:
  0.0 29.3 %collective-permute-start.2 = (bf16[256,2048]{1,0:T(8,128)(2,1)}, bf16[256,2048]{1,0:T(8,128)(2,1)S(1)}, u32[]{:S(2)}, u32[]{:S(2)}) collective-permute-start(bf16[256,2048]{1,0:T(8,128)(2,1)} %own_ref.1), channel_id=1, source_target_pairs={{0,1},{1,2},{2,3},{3,0},{4,7},{5,4},{6,5},{7,6},{8,9},{9,10},{10,1... | collective-permute-start | bytes 3145736 | tf_op jit(solution)/shard_map/ppermute | solution.py:285
  4.5 22.6 %collective-permute-start.1 = (bf16[16,256]{1,0:T(8,128)(2,1)S(1)}, bf16[16,256]{1,0:T(8,128)(2,1)S(1)}, u32[]{:S(2)}, u32[]{:S(2)}) collective-permute-start(bf16[16,256]{1,0:T(8,128)(2,1)S(1)} %get-tuple-element.25), channel_id=1, source_target_pairs={{4,0},{8,4},{12,8},{16,12},{20,16},{24,20},{28,24},{32,28},{36,32}... | collective-permute-start | bytes 24584 | tf_op jit(solution)/shard_map/ppermute | solution.py:274
  23.1 4.0 %collective-permute-start = (bf16[16,256]{1,0:T(8,128)(2,1)S(1)}, bf16[16,256]{1,0:T(8,128)(2,1)S(1)}, u32[]{:S(2)}, u32[]{:S(2)}) collective-permute-start(bf16[16,256]{1,0:T(8,128)(2,1)S(1)} %get-tuple-element.26), channel_id=1, source_target_pairs={{0,4},{4,8},{8,12},{12,16},{16,20},{20,24},{24,28},{28,32},{32,36}... | collective-permute-start | bytes 24584 | tf_op jit(solution)/shard_map/ppermute | solution.py:273
  27.1 23.9 %copy-start.6 = (s32[128,2]{0,1:T(2,128)S(1)}, s32[128,2]{0,1:T(2,128)}, u32[]{:S(2)}) copy-start(s32[128,2]{0,1:T(2,128)} %param.19) | copy-start | bytes 3076
  27.1 23.9 %copy-start.7 = (f32[128,2]{0,1:T(2,128)S(1)}, f32[128,2]{0,1:T(2,128)}, u32[]{:S(2)}) copy-start(f32[128,2]{0,1:T(2,128)} %param.20) | copy-start | bytes 3076
  29.3 28.6 %collective-permute-start.3 = (bf16[256,2048]{1,0:T(8,128)(2,1)S(1)}, bf16[256,2048]{1,0:T(8,128)(2,1)}, u32[]{:S(2)}, u32[]{:S(2)}) collective-permute-start(bf16[256,2048]{1,0:T(8,128)(2,1)S(1)} %collective-permute-done.2.near_ref), channel_id=1, source_target_pairs={{0,4},{4,0},{8,12},{12,8},{16,20},{20,16},{24,28},{28,24},{32,36},... | collective-permute-start | bytes 3145736 | tf_op jit(solution)/shard_map/ppermute | solution.py:300
  36.7 21.2 %copy-start.3 = (bf16[256,2048]{1,0:T(8,128)(2,1)S(1)}, bf16[256,2048]{1,0:T(8,128)(2,1)}, u32[]{:S(2)}) copy-start(bf16[256,2048]{1,0:T(8,128)(2,1)} %own_ref.1) | copy-start | bytes 3145732
  36.7 8.5 %collective-permute-start.4 = (bf16[128,2048]{1,0:T(8,128)(2,1)S(1)}, bf16[128,2048]{1,0:T(8,128)(2,1)}, u32[]{:S(2)}, u32[]{:S(2)}) collective-permute-start(bf16[128,2048]{1,0:T(8,128)(2,1)S(1)} %constant_dynamic-slice_fusion), channel_id=1, source_target_pairs={{0,1},{1,2},{2,3},{3,0},{4,7},{5,4},{6,5},{7,6},{8,9},{9,10},{10,1... | collective-permute-start | bytes 1572872 | tf_op jit(solution)/shard_map/ppermute | solution.py:299
  45.2 15.1 %collective-permute-start.5 = (bf16[128,2048]{1,0:T(8,128)(2,1)}, bf16[128,2048]{1,0:T(8,128)(2,1)}, u32[]{:S(2)}, u32[]{:S(2)}) collective-permute-start(bf16[128,2048]{1,0:T(8,128)(2,1)} %collective-permute-done.4.half_ref), channel_id=1, source_target_pairs={{0,4},{4,0},{8,12},{12,8},{16,20},{20,16},{24,28},{28,24},{32,36},... | collective-permute-start | bytes 1572872 | tf_op jit(solution)/shard_map/ppermute | solution.py:301
  47.3 10.6 %all-to-all-start = ((bf16[4,144,256]{2,1,0:T(8,128)(2,1)}), bf16[4,144,256]{2,1,0:T(8,128)(2,1)S(1)}, u32[]{:S(2)}, u32[]{:S(2)}) async-start(bf16[4,144,256]{2,1,0:T(8,128)(2,1)} %shard_map.118), calls=%async_computation | async-start | bytes 589824 | tf_op jit(solution)/shard_map/all_to_all | solution.py:302
  51.9 0.8 copy-start.8
  52.7 7.7 %copy-start.5 = (f32[2048]{0:T(1024)S(1)}, f32[2048]{0:T(1024)}, u32[]{:S(2)}) copy-start(f32[2048]{0:T(1024)} %param.18) | copy-start | bytes 24580
  57.9 2.5 copy-start.4
  57.9 2.5 copy-start.9
  57.9 112.4 %copy-start.2 = (bf16[1,768,2048]{2,1,0:T(8,128)(2,1)S(1)}, bf16[1,768,2048]{2,1,0:T(8,128)(2,1)}, u32[]{:S(2)}) copy-start(bf16[1,768,2048]{2,1,0:T(8,128)(2,1)} %param.23) | copy-start | bytes 9437188
  60.4 109.9 %copy-start.1 = (bf16[1,2048,768]{2,1,0:T(8,128)(2,1)S(1)}, bf16[1,2048,768]{2,1,0:T(8,128)(2,1)}, u32[]{:S(2)}) copy-start(bf16[1,2048,768]{2,1,0:T(8,128)(2,1)} %param.22) | copy-start | bytes 9437188
  63.0 107.3 %copy-start = (bf16[1,2048,768]{2,1,0:T(8,128)(2,1)S(1)}, bf16[1,2048,768]{2,1,0:T(8,128)(2,1)}, u32[]{:S(2)}) copy-start(bf16[1,2048,768]{2,1,0:T(8,128)(2,1)} %param.21) | copy-start | bytes 9437188

commit v5 on v4

--- a/solution.py
+++ b/solution.py
@@ -114,6 +114,11 @@
             factor_ref[first : first + rows] = jnp.where(here, value, 0.0).astype(BF16)
 
 
+def half_kernel(place_ref, block_ref, out_ref):
+    rows = out_ref.shape[0]
+    out_ref[...] = block_ref[pl.ds(pl.multiple_of(place_ref[1] * rows, rows), rows)]
+
+
 def partial_kernel(
     place_ref, mixed_ref, own_ref, near_ref, swapped_ref, out_ref, first_ref, second_ref, value_ref, act_ref
 ):
@@ -295,7 +300,10 @@
         10**9, 8,
     )(gated, low, high, table)
     near, _ = lax.optimization_barrier((near, sent))
-    half = lax.dynamic_slice_in_dim(near, core * half_width, half_width, 0)
+    whereabouts = jnp.stack([place, core])
+    half = call(half_kernel, [SMEM, VMEM], shape((half_width, features), BF16), [], 10**6, 4)(
+        whereabouts, near
+    )
     half = lax.ppermute(half, ("sp", "tp"), aside)
     swapped = lax.ppermute(near, "sp", swap)
     rest = lax.ppermute(half, "sp", swap)
@@ -312,7 +320,7 @@
         [shape((rows, features), F32)] + [shape((rows, half_width), BF16)] * 2,
         [pltpu.VMEM((owners, rows, width), F32), pltpu.VMEM((owners, rows, width), BF16)],
         10**9, 8,
-    )(jnp.stack([place, core]), mixed, point_weight, near, swapped)
+    )(whereabouts, mixed, point_weight, near, swapped)
     after, box = call(
         dispatch_kernel, [VMEM] * 8,
         [shape((rows, features), BF16), shape((experts * PACK, span), BF16)],

time: 286 us -> 287 us (level)
  no operation moved by 1% of the time
where the time goes in v5:
time: 287 us
  blocking collectives  215 us (75%)
  starting transfers between devices  37.4 us (13%)
  Pallas kernels  16.9 us (6%)
  waiting for transfers between devices  13.7 us (5%)
    all_to_all x1, blocking collectives, shards(): lax.all_to_all(answer, ('sp', 'tp'), split_axis=0, concat_axis=0, tiled=T...  107 us
    all_to_all x1, blocking collectives, shards(): lax.all_to_all(box, ('sp', 'tp'), split_axis=0, concat_axis=0, tiled=True)  107 us
    ppermute x1, starting transfers between devices, shards(): high = lax.ppermute(gate(conv_value[:HALO], conv_gate[:HALO]), 'sp', behind)  18.7 us
    ppermute x1, waiting for transfers between devices, shards(): half = lax.ppermute(half, ('sp', 'tp'), aside)  8.4 us
    ppermute x1, starting transfers between devices, shards(): swapped = lax.ppermute(near, 'sp', swap)  7.36 us
    pallas_call x1, Pallas kernels, shards(): call(expert_kernel, [VMEM] * 4, shape((members * PACK, span), BF16), [plt...  6.15 us
  transfers between devices with their start and end apart: 7, of which 2 were waited for; matrix products, arithmetic and copies ran while one was open for 1% of the time, Pallas kernels for 2%

profile of v5, /device:TPU:33, one launch (start us, length us, event | category | flops | bytes accessed | tf_op | source)
XLA Modules:
  0.0 286.6 jit_solution(12150660808994354190)
XLA Ops:
  0.0 3.7 %collective-permute-start.2 = (bf16[256,2048]{1,0:T(8,128)(2,1)}, bf16[256,2048]{1,0:T(8,128)(2,1)S(1)}, u32[]{:S(2)}, u32[]{:S(2)}) collective-permute-start(bf16[256,2048]{1,0:T(8,128)(2,1)} %own_ref.1), channel_id=1, source_target_pairs={{0,1},{1,2},{2,3},{3,0},{4,7},{5,4},{6,5},{7,6},{8,9},{9,10},{10,1... | collective-permute-start | bytes 3145736 | tf_op jit(solution)/shard_map/ppermute | solution.py:290
  3.7 0.8 multiply_convert_fusion.1
  4.5 18.7 %collective-permute-start.1 = (bf16[16,256]{1,0:T(8,128)(2,1)S(1)}, bf16[16,256]{1,0:T(8,128)(2,1)S(1)}, u32[]{:S(2)}, u32[]{:S(2)}) collective-permute-start(bf16[16,256]{1,0:T(8,128)(2,1)S(1)} %get-tuple-element.25), channel_id=1, source_target_pairs={{4,0},{8,4},{12,8},{16,12},{20,16},{24,20},{28,24},{32,28},{36,32}... | collective-permute-start | bytes 24584 | tf_op jit(solution)/shard_map/ppermute | solution.py:279
  23.1 2.0 collective-permute-start
  25.1 1.2 multiply_convert_fusion.rows_ref
  26.3 0.8 pad_maximum_fusion.table_ref
  27.1 0.0 copy-start.6
  27.1 0.0 copy-start.7
  27.1 0.0 collective-permute-done.1.high_ref
  27.1 0.0 collective-permute-done.low_ref
  27.1 2.2 shard_map.118
  29.3 0.0 collective-permute-done.2.near_ref.block_ref
  29.3 7.4 %collective-permute-start.3 = (bf16[256,2048]{1,0:T(8,128)(2,1)S(1)}, bf16[256,2048]{1,0:T(8,128)(2,1)}, u32[]{:S(2)}, u32[]{:S(2)}) collective-permute-start(bf16[256,2048]{1,0:T(8,128)(2,1)S(1)} %collective-permute-done.2.near_ref.block_ref), channel_id=1, source_target_pairs={{0,4},{4,0},{8,12},{12,8},{16,20},{20,16},{24,28},{28,24},{32,36},... | collective-permute-start | bytes 3145736 | tf_op jit(solution)/shard_map/ppermute | solution.py:308
  36.6 0.1 pad_add_fusion.place_ref
  36.7 0.6 shard_map.120
  37.3 0.0 copy-start.3
  37.3 0.1 collective-permute-start.4
  37.4 8.4 %collective-permute-done.4.half_ref = bf16[128,2048]{1,0:T(8,128)(2,1)} collective-permute-done((bf16[128,2048]{1,0:T(8,128)(2,1)S(1)}, bf16[128,2048]{1,0:T(8,128)(2,1)}, u32[]{:S(2)}, u32[]{:S(2)}) %collective-permute-start.4) | collective-permute-done | bytes 524320 | tf_op jit(solution)/shard_map/ppermute | solution.py:307
  45.9 2.1 collective-permute-start.5
  47.9 3.5 %all-to-all-start = ((bf16[4,144,256]{2,1,0:T(8,128)(2,1)}), bf16[4,144,256]{2,1,0:T(8,128)(2,1)S(1)}, u32[]{:S(2)}, u32[]{:S(2)}) async-start(bf16[4,144,256]{2,1,0:T(8,128)(2,1)} %shard_map.118), calls=%async_computation | async-start | bytes 589824 | tf_op jit(solution)/shard_map/all_to_all | solution.py:310
  51.5 0.0 copy-done.6
  51.5 0.0 copy-done.7
  51.5 0.9 shard_map.121
  52.4 0.0 copy-start.8
  52.4 0.8 copy-done.8
  53.2 0.0 copy-start.5
  53.2 5.3 %all-to-all-done.mixed_ref = bf16[4,144,256]{2,1,0:T(8,128)(2,1)S(1)} async-done(((bf16[4,144,256]{2,1,0:T(8,128)(2,1)}), bf16[4,144,256]{2,1,0:T(8,128)(2,1)S(1)}, u32[]{:S(2)}, u32[]{:S(2)}) %all-to-all-start) | async-done | bytes 294944 | tf_op jit(solution)/shard_map/all_to_all | solution.py:310
  58.5 0.0 copy-start.4
  58.5 0.0 copy-start.9
  58.5 0.0 collective-permute-done.3.swapped_ref
  58.5 0.0 copy-done.3
  58.5 0.0 copy-start.2
  58.5 2.4 shard_map.119
  61.0 0.0 collective-permute-done.5.rest_ref
  61.0 0.0 copy-done.5
  61.0 0.0 copy-done.4
  61.0 0.0 copy-done.9
  61.0 0.0 copy-start.1
  61.0 2.6 shard_map.122
  63.6 0.0 copy-start
  63.7 107.3 %all_to_all.15 = bf16[128,8,1024]{2,1,0:T(8,128)(2,1)S(1)} all-to-all(bf16[128,8,1024]{2,1,0:T(8,128)(2,1)S(1)} %bitcast.14), channel_id=1, replica_groups=mesh['grp'=2,'sp'=32,'tp'=4] {'sp','tp'}, dimensions={0} | all-to-all | bytes 4194304 | tf_op jit(solution)/shard_map/all_to_all | solution.py:331
  170.9 0.0 copy-done.2
  170.9 0.0 copy-done.1
  170.9 0.0 copy-done
  170.9 6.2 %shard_map.123 = bf16[1024,1024]{1,0:T(8,128)(2,1)S(1)} custom-call(bf16[1024,1024]{1,0:T(8,128)(2,1)S(1)} %bitcast.15, bf16[2048,768]{1,0:T(8,128)(2,1)S(1)} %bitcast.17, bf16[2048,768]{1,0:T(8,128)(2,1)S(1)} %bitcast.18, bf16[768,2048]{1,0:T(8,128)(2,1)S(1)} %bitcast.19), custom_call_target="tpu_custom_call" | custom-call | flops 5000000000 | bytes 1048576 | tf_op jit(solution)/shard_map/pallas_call | solution.py:333
  177.1 107.5 %all_to_all.16 = bf16[128,8,1024]{2,1,0:T(8,128)(2,1)S(1)} all-to-all(bf16[128,8,1024]{2,1,0:T(8,128)(2,1)S(1)} %bitcast.16), channel_id=1, replica_groups=mesh['grp'=2,'sp'=32,'tp'=4] {'sp','tp'}, dimensions={0} | all-to-all | bytes 4194304 | tf_op jit(solution)/shard_map/all_to_all | solution.py:343
  284.6 2.0 shard_map.124
Async XLA Ops:
  0.0 29.3 %collective-permute-start.2 = (bf16[256,2048]{1,0:T(8,128)(2,1)}, bf16[256,2048]{1,0:T(8,128)(2,1)S(1)}, u32[]{:S(2)}, u32[]{:S(2)}) collective-permute-start(bf16[256,2048]{1,0:T(8,128)(2,1)} %own_ref.1), channel_id=1, source_target_pairs={{0,1},{1,2},{2,3},{3,0},{4,7},{5,4},{6,5},{7,6},{8,9},{9,10},{10,1... | collective-permute-start | bytes 3145736 | tf_op jit(solution)/shard_map/ppermute | solution.py:290
  4.5 22.6 %collective-permute-start.1 = (bf16[16,256]{1,0:T(8,128)(2,1)S(1)}, bf16[16,256]{1,0:T(8,128)(2,1)S(1)}, u32[]{:S(2)}, u32[]{:S(2)}) collective-permute-start(bf16[16,256]{1,0:T(8,128)(2,1)S(1)} %get-tuple-element.25), channel_id=1, source_target_pairs={{4,0},{8,4},{12,8},{16,12},{20,16},{24,20},{28,24},{32,28},{36,32}... | collective-permute-start | bytes 24584 | tf_op jit(solution)/shard_map/ppermute | solution.py:279
  23.1 4.0 %collective-permute-start = (bf16[16,256]{1,0:T(8,128)(2,1)S(1)}, bf16[16,256]{1,0:T(8,128)(2,1)S(1)}, u32[]{:S(2)}, u32[]{:S(2)}) collective-permute-start(bf16[16,256]{1,0:T(8,128)(2,1)S(1)} %get-tuple-element.26), channel_id=1, source_target_pairs={{0,4},{4,8},{8,12},{12,16},{16,20},{20,24},{24,28},{28,32},{32,36}... | collective-permute-start | bytes 24584 | tf_op jit(solution)/shard_map/ppermute | solution.py:278
  27.1 24.4 %copy-start.6 = (s32[128,2]{0,1:T(2,128)S(1)}, s32[128,2]{0,1:T(2,128)}, u32[]{:S(2)}) copy-start(s32[128,2]{0,1:T(2,128)} %param.19) | copy-start | bytes 3076
  27.1 24.4 %copy-start.7 = (f32[128,2]{0,1:T(2,128)S(1)}, f32[128,2]{0,1:T(2,128)}, u32[]{:S(2)}) copy-start(f32[128,2]{0,1:T(2,128)} %param.20) | copy-start | bytes 3076
  29.3 29.2 %collective-permute-start.3 = (bf16[256,2048]{1,0:T(8,128)(2,1)S(1)}, bf16[256,2048]{1,0:T(8,128)(2,1)}, u32[]{:S(2)}, u32[]{:S(2)}) collective-permute-start(bf16[256,2048]{1,0:T(8,128)(2,1)S(1)} %collective-permute-done.2.near_ref.block_ref), channel_id=1, source_target_pairs={{0,4},{4,0},{8,12},{12,8},{16,20},{20,16},{24,28},{28,24},{32,36},... | collective-permute-start | bytes 3145736 | tf_op jit(solution)/shard_map/ppermute | solution.py:308
  37.3 21.2 %copy-start.3 = (bf16[256,2048]{1,0:T(8,128)(2,1)S(1)}, bf16[256,2048]{1,0:T(8,128)(2,1)}, u32[]{:S(2)}) copy-start(bf16[256,2048]{1,0:T(8,128)(2,1)} %own_ref.1) | copy-start | bytes 3145732
  37.3 8.5 %collective-permute-start.4 = (bf16[128,2048]{1,0:T(8,128)(2,1)S(1)}, bf16[128,2048]{1,0:T(8,128)(2,1)}, u32[]{:S(2)}, u32[]{:S(2)}) collective-permute-start(bf16[128,2048]{1,0:T(8,128)(2,1)S(1)} %shard_map.120), channel_id=1, source_target_pairs={{0,1},{1,2},{2,3},{3,0},{4,7},{5,4},{6,5},{7,6},{8,9},{9,10},{10,1... | collective-permute-start | bytes 1572872 | tf_op jit(solution)/shard_map/ppermute | solution.py:307
  45.9 15.1 %collective-permute-start.5 = (bf16[128,2048]{1,0:T(8,128)(2,1)}, bf16[128,2048]{1,0:T(8,128)(2,1)}, u32[]{:S(2)}, u32[]{:S(2)}) collective-permute-start(bf16[128,2048]{1,0:T(8,128)(2,1)} %collective-permute-done.4.half_ref), channel_id=1, source_target_pairs={{0,4},{4,0},{8,12},{12,8},{16,20},{20,16},{24,28},{28,24},{32,36},... | collective-permute-start | bytes 1572872 | tf_op jit(solution)/shard_map/ppermute | solution.py:309
  47.9 10.6 %all-to-all-start = ((bf16[4,144,256]{2,1,0:T(8,128)(2,1)}), bf16[4,144,256]{2,1,0:T(8,128)(2,1)S(1)}, u32[]{:S(2)}, u32[]{:S(2)}) async-start(bf16[4,144,256]{2,1,0:T(8,128)(2,1)} %shard_map.118), calls=%async_computation | async-start | bytes 589824 | tf_op jit(solution)/shard_map/all_to_all | solution.py:310
  52.4 0.8 copy-start.8
  53.2 7.8 %copy-start.5 = (f32[2048]{0:T(1024)S(1)}, f32[2048]{0:T(1024)}, u32[]{:S(2)}) copy-start(f32[2048]{0:T(1024)} %param.18) | copy-start | bytes 24580
  58.5 2.5 copy-start.4
  58.5 2.5 copy-start.9
  58.5 112.4 %copy-start.2 = (bf16[1,768,2048]{2,1,0:T(8,128)(2,1)S(1)}, bf16[1,768,2048]{2,1,0:T(8,128)(2,1)}, u32[]{:S(2)}) copy-start(bf16[1,768,2048]{2,1,0:T(8,128)(2,1)} %param.23) | copy-start | bytes 9437188
  61.0 109.9 %copy-start.1 = (bf16[1,2048,768]{2,1,0:T(8,128)(2,1)S(1)}, bf16[1,2048,768]{2,1,0:T(8,128)(2,1)}, u32[]{:S(2)}) copy-start(bf16[1,2048,768]{2,1,0:T(8,128)(2,1)} %param.22) | copy-start | bytes 9437188
  63.6 107.3 %copy-start = (bf16[1,2048,768]{2,1,0:T(8,128)(2,1)S(1)}, bf16[1,2048,768]{2,1,0:T(8,128)(2,1)}, u32[]{:S(2)}) copy-start(bf16[1,2048,768]{2,1,0:T(8,128)(2,1)} %param.21) | copy-start | bytes 9437188
